TPU v7x, 32 devices: a whole 2x2x4 slice. The times are simulated.
32 devices in a mesh: sp: 16 (over z, y, core), tp: 2 (over x).
Axes of the slice: x: 2, y: 2, z: 4, core: 2. Of those that a mesh axis runs over, the one named last changes fastest.
Arguments:
- tokens: bfloat16 [4096, 2048], P(('sp', 'tp')), may hold values from -96 to 96
- norm_gain: float32 [2048], replicated, may hold values from 0.1 to 1.9
- w_query: bfloat16 [2048, 1024], P(None, 'tp'), may hold values from -0.3 to 0.3
- w_key: bfloat16 [2048, 1024], P(None, 'tp'), may hold values from -0.3 to 0.3
- w_value: bfloat16 [2048, 1024], P(None, 'tp'), may hold values from -0.125 to 0.125
- w_att_gate: bfloat16 [2048, 1024], P(None, 'tp'), may hold values from -0.125 to 0.125
- w_rec_in: bfloat16 [2048, 1024], P(None, 'tp'), may hold values from -0.125 to 0.125
- w_rec_gate: bfloat16 [2048, 1024], P(None, 'tp'), may hold values from -0.125 to 0.125
- conv_taps: float32 [4, 1024], P(None, 'tp'), may hold values from -3 to 3
- gate_recur: bfloat16 [8, 128, 128], P('tp'), may hold values from -0.5 to 0.5
- gate_input: bfloat16 [8, 128, 128], P('tp'), may hold values from -0.5 to 0.5
- decay_rate: float32 [1024], P('tp'), may hold values from 1e-06 to 0.02
- head_lambda: float32 [8], P('tp'), may hold values from 0.3 to 0.8
- head_gain: float32 [1024], P('tp'), may hold values from 0.1 to 1.9
- out_att: bfloat16 [1024, 2048], P('tp'), may hold values from -0.125 to 0.125
- out_rec: bfloat16 [1024, 2048], P('tp'), may hold values from -0.125 to 0.125
Outputs:
- layer_out: bfloat16 [4096, 2048], P(('sp', 'tp'))
All inputs are finite; a program needn't handle non-finite values.
Results may differ from a plain program's by a relative error of at most 0.015.
Values may be sent and summed in bfloat16 or wider, within the bound.
A program may use at most 128 MiB of HBM per device.

v0:
```python
import math

import jax
import jax.numpy as jnp
from jax import lax
from jax.sharding import PartitionSpec as P

EPS_INPUT = 1e-06
EPS_HEAD = 1e-05
RATE_SCALE = 8.0
HEAD_FACTOR = 0.8
MASKED = -1e30


def passed_along(block, axis, distance):
    devices = range(lax.axis_size(axis))
    route = [(i - distance, i) for i in devices if i - distance in devices]
    return lax.ppermute(block, axis, route)


def carried_in(value, axis, join, neutral):
    count, mine = (lax.axis_size(axis), lax.axis_index(axis))
    pieces = jax.tree.map(lambda part: lax.all_gather(part, axis), value)
    subtotal = jax.tree.map(
        lambda part, zero: jnp.full_like(part, 0) + jnp.asarray(zero, part.dtype), value, neutral
    )

    def hop(position, subtotal):
        longer = join(subtotal, jax.tree.map(lambda part: part[position], pieces))
        return jax.tree.map(lambda new, old: jnp.where(position < mine, new, old), longer, subtotal)

    return lax.fori_loop(0, count - 1, hop, subtotal)


def rms_rows(values, gain, epsilon):
    mean_square = jnp.mean(values * values, axis=-1, keepdims=True)
    return values * lax.rsqrt(mean_square + epsilon) * gain


def combine_pair(earlier, later):
    return (earlier[0] * later[0], later[0] * earlier[1] + later[1])


def attention(queries, keys, values, head_lambda, head_gain, att_gate):
    rows = queries.shape[0]
    local_heads = head_lambda.shape[0]
    head_dim = queries.shape[1] // (2 * local_heads)
    value_dim = values.shape[1] // local_heads
    scale = head_dim ** (-0.5)
    query_heads = queries.reshape(rows, local_heads, 2, head_dim)
    query_pos = lax.axis_index("sp") * rows + jnp.arange(rows, dtype=jnp.int32)
    initial = (
        jnp.full((2, local_heads, rows), MASKED, jnp.float32),
        jnp.zeros((2, local_heads, rows), jnp.float32),
        jnp.zeros((2, local_heads, rows, value_dim), jnp.float32),
    )
    running = initial
    key_piece = lax.all_gather(keys, "sp", axis=0, tiled=True)
    value_piece = lax.all_gather(values, "sp", axis=0, tiled=True)
    length = key_piece.shape[0]
    block_len = math.gcd(length, 512)
    block_count = length // block_len
    key_blocks = key_piece.reshape(block_count, block_len, local_heads, 2, head_dim)
    value_blocks = value_piece.reshape(block_count, block_len, local_heads, value_dim)
    block_starts = block_len * jnp.arange(block_count, dtype=jnp.int32)

    def one_block(current, inputs):
        key_block, value_block, block_start = inputs
        highest, totals, weighted = current
        key_pos = block_start + jnp.arange(block_len, dtype=jnp.int32)
        allowed = key_pos[None, :] <= query_pos[:, None]
        scores = (
            jnp.einsum(
                "qhpd,khpd->phqk", query_heads, key_block, preferred_element_type=jnp.float32
            )
            * scale
        )
        scores = jnp.where(allowed, scores, MASKED)
        new_high = jnp.maximum(highest, jnp.max(scores, axis=-1))
        factor = jnp.exp(highest - new_high)
        raised = jnp.where(allowed, jnp.exp(scores - new_high[..., None]), 0.0)
        totals = totals * factor + jnp.sum(raised, axis=-1)
        weighted = weighted * factor[..., None] + jnp.einsum(
            "phqk,khe->phqe",
            raised.astype(jnp.bfloat16),
            value_block,
            preferred_element_type=jnp.float32,
        )
        return ((new_high, totals, weighted), None)

    running, _ = lax.scan(one_block, running, (key_blocks, value_blocks, block_starts))
    highest, totals, weighted = running
    normalized = weighted / totals[..., None]
    per_head = normalized[0] - head_lambda[:, None, None] * normalized[1]
    head_out = (
        rms_rows(per_head, head_gain.reshape(local_heads, 1, value_dim), EPS_HEAD) * HEAD_FACTOR
    )
    head_out = jnp.moveaxis(head_out, 0, 1).reshape(rows, local_heads * value_dim)
    return (head_out * jax.nn.silu(att_gate.astype(jnp.float32))).astype(jnp.bfloat16)


def recurrence(rec_in, rec_gate, conv_taps, gate_recur, gate_input, decay_rate):
    rows, width = rec_in.shape
    taps = conv_taps.shape[0]
    earlier = passed_along(rec_in[rows - (taps - 1) :], "sp", 1)
    padded = jnp.concatenate([earlier, rec_in], axis=0).astype(jnp.float32)
    conv_sum = jnp.zeros((rows, width), jnp.float32)
    for offset in range(taps):
        conv_sum = conv_sum + padded[offset : offset + rows] * conv_taps[offset]
    conv_out = conv_sum.astype(jnp.bfloat16)
    local_blocks = gate_recur.shape[0]
    grouped = conv_out.reshape(rows, local_blocks, gate_recur.shape[1])
    recur_gate = jax.nn.sigmoid(
        jnp.einsum("tnc,ncd->tnd", grouped, gate_recur, preferred_element_type=jnp.float32).reshape(
            rows, width
        )
    )
    inflow = jax.nn.sigmoid(
        jnp.einsum("tnc,ncd->tnd", grouped, gate_input, preferred_element_type=jnp.float32).reshape(
            rows, width
        )
    )
    log_decay = -RATE_SCALE * recur_gate * decay_rate
    decays = jnp.exp(log_decay)
    positions = lax.axis_index("sp") * rows + jnp.arange(rows, dtype=jnp.int32)
    norm_in = jnp.where((positions == 0)[:, None], 1.0, jnp.sqrt(-jnp.expm1(2.0 * log_decay)))
    driven = norm_in * inflow * conv_out.astype(jnp.float32)
    products, partial_states = lax.associative_scan(combine_pair, (decays, driven), axis=0)
    identity = (jnp.ones((width,), jnp.float32), jnp.zeros((width,), jnp.float32))
    incoming = carried_in(
        (products[rows - 1], partial_states[rows - 1]), "sp", combine_pair, identity
    )
    states = partial_states + products * incoming[1][None, :]
    return (states * jax.nn.silu(rec_gate.astype(jnp.float32))).astype(jnp.bfloat16)


def body(
    tokens,
    norm_gain,
    w_query,
    w_key,
    w_value,
    w_att_gate,
    w_rec_in,
    w_rec_gate,
    conv_taps,
    gate_recur,
    gate_input,
    decay_rate,
    head_lambda,
    head_gain,
    out_att,
    out_rec,
):
    normed = rms_rows(tokens.astype(jnp.float32), norm_gain, EPS_INPUT).astype(jnp.bfloat16)
    weights = (w_query, w_key, w_value, w_att_gate, w_rec_in, w_rec_gate)
    joined = jnp.concatenate(weights, axis=1)
    projected = jnp.dot(
        lax.all_gather(normed, "tp", axis=0, tiled=True), joined, preferred_element_type=jnp.float32
    ).astype(jnp.bfloat16)
    bounds = [0]
    for weight in weights:
        bounds.append(bounds[-1] + weight.shape[1])
    queries, keys, values, att_gate, rec_in, rec_gate = [
        projected[:, bounds[index] : bounds[index + 1]] for index in range(6)
    ]
    att_mixed = attention(queries, keys, values, head_lambda, head_gain, att_gate)
    rec_mixed = recurrence(rec_in, rec_gate, conv_taps, gate_recur, gate_input, decay_rate)
    att_rows, rec_rows = (
        lax.all_to_all(att_mixed, "tp", split_axis=0, concat_axis=1, tiled=True),
        lax.all_to_all(rec_mixed, "tp", split_axis=0, concat_axis=1, tiled=True),
    )
    att_whole, rec_whole = (
        lax.all_gather(out_att, "tp", axis=0, tiled=True),
        lax.all_gather(out_rec, "tp", axis=0, tiled=True),
    )
    total = jnp.dot(att_rows, att_whole, preferred_element_type=jnp.float32) + jnp.dot(
        rec_rows, rec_whole, preferred_element_type=jnp.float32
    )
    return total.astype(jnp.bfloat16)


def solution(mesh):
    return jax.shard_map(
        body,
        mesh=mesh,
        in_specs=(
            P(("sp", "tp"), None),
            P(),
            P(None, "tp"),
            P(None, "tp"),
            P(None, "tp"),
            P(None, "tp"),
            P(None, "tp"),
            P(None, "tp"),
            P(None, "tp"),
            P("tp", None, None),
            P("tp", None, None),
            P("tp"),
            P("tp"),
            P("tp"),
            P("tp", None),
            P("tp", None),
        ),
        out_specs=P(("sp", "tp"), None),
        check_vma=False,
    )
```

profile of v0, /device:TPU:0, one launch (start us, length us, event | category | flops | bytes accessed | tf_op | source)
XLA Modules:
  0.0 298.5 jit_solution(3188231626033430947)
XLA Ops:
  7.9 2.0 fusion.28
  10.0 3.3 %constant_dynamic-update-slice_fusion.5 = bf16[2048,3072]{1,0:T(8,128)(2,1)} fusion(bf16[2048,512]{1,0:T(8,128)(2,1)} %param.22), kind=kLoop, calls=%fused_computation.116 | loop fusion | bytes 4194304
  13.3 1.6 constant_dynamic-update-slice_fusion.4
  15.0 1.6 constant_dynamic-update-slice_fusion.3
  16.6 1.6 constant_dynamic-update-slice_fusion.2
  18.2 1.6 constant_dynamic-update-slice_fusion.1
  19.7 1.6 constant_dynamic-update-slice_fusion
  21.4 12.8 %all-gather.8.cloned.1.call-done = bf16[256,2048]{1,0:T(8,128)(2,1)} async-done(((bf16[128,2048]{1,0:T(8,128)(2,1)}), bf16[256,2048]{1,0:T(8,128)(2,1)}) %all-gather.8.cloned.1.call-update) | async-done | bytes 1048592 | tf_op jit(solution)/shard_map/all_gather | solution.py:159
  34.1 8.3 %convolution_convert_fusion = bf16[256,3072]{1,0:T(8,128)(2,1)S(1)} fusion(bf16[256,2048]{1,0:T(8,128)(2,1)} %all-gather.8.cloned.1.call-done, bf16[2048,3072]{1,0:T(8,128)(2,1)} %constant_dynamic-update-slice_fusion), kind=kOutput, calls=%fused_computation.27 | convolution fusion | flops 3222011904 | bytes 15204352 | tf_op jit(solution)/shard_map/dot_general | solution.py:158
  46.1 1.6 collective-permute-start
  56.1 24.3 %all-gather.1 = f32[16,1,512]{2,1,0:T(1,128)S(1)} all-gather(f32[1,1,512]{2,1,0:T(1,128)S(1)} %add_bitcast_fusion), channel_id=1, replica_groups=mesh['sp'=16,'tp'=2] {'sp'}, dimensions={0}, use_global_device_ids=true | all-gather | bytes 34816 | tf_op jit(solution)/shard_map/all_gather | solution.py:23
  80.6 17.9 %all-gather = f32[16,1,512]{2,1,0:T(1,128)S(1)} all-gather(f32[1,1,512]{2,1,0:T(1,128)S(1)} %add_bitcast_fusion.1), channel_id=1, replica_groups=mesh['sp'=16,'tp'=2] {'sp'}, dimensions={0}, use_global_device_ids=true | all-gather | bytes 34816 | tf_op jit(solution)/shard_map/all_gather | solution.py:23
  99.4 16.1 %reshape.80 = bf16[8,512,4,2,64]{4,3,2,1,0:T(2,128)(2,1)} reshape(bf16[4096,512]{1,0:T(8,128)(2,1)} %all-gather.10.cloned.1.call-done) | data formatting | bytes 8388608 | tf_op jit(solution)/shard_map/reshape | solution.py:63
  115.5 20.2 %copy.53 = bf16[8,512,4,2,64]{1,4,2,3,0:T(8,128)(2,1)} copy(bf16[8,512,4,2,64]{4,3,2,1,0:T(2,128)(2,1)} %reshape.80) | data formatting | bytes 8388608
  135.7 9.8 %all-gather.12.cloned.1.call-done = bf16[4096,512]{1,0:T(8,128)(2,1)} async-done(((bf16[256,512]{1,0:T(8,128)(2,1)}), bf16[4096,512]{1,0:T(8,128)(2,1)}) %all-gather.12.cloned.1.call-update) | async-done | bytes 4194320 | tf_op jit(solution)/shard_map/all_gather | solution.py:59
  145.5 7.0 %reshape.72 = bf16[8,512,4,128]{3,2,1,0:T(4,128)(2,1)} reshape(bf16[4096,512]{1,0:T(8,128)(2,1)} %all-gather.12.cloned.1.call-done) | data formatting | bytes 8388608 | tf_op jit(solution)/shard_map/reshape | solution.py:64
  152.5 112.2 %while.29 = (s32[]{:T(128)}, f32[2,4,256]{2,1,0:T(4,128)S(1)}, f32[2,4,256]{2,1,0:T(4,128)S(1)}, f32[2,4,256,128]{2,3,0,1:T(8,128)}, s32[8]{0:T(128)}, /*index=5...) while((s32[]{:T(128)}, f32[2,4,256]{2,1,0:T(4,128)S(1)}, ...), condition=%wide.region_4.5_spmd.clone, body=%wide.region_1.4_spmd.clone.sunk | while | flops 413018880 | bytes 18692808 | solution.py:91
  154.6 3.9 %fusion.84 = (f32[2,4,256]{2,1,0:T(4,128)S(1)}, f32[2,4,512,256]{3,2,1,0:T(8,128)}) fusion(pred[256,512]{0,1:T(8,128)(4,1)S(1)} %broadcast_compare_fusion.2, bf16[256,4,2,64]{0,3,1,2:T(8,128)(2,1)S(1)} %get-tuple-element.465, bf16[8,512,4,2,64]{1,4,2,3,0:T(8,128)(2,1)} %get-tuple-element.464, s32[]{:T(128)} %get-tuple-element.448), kind=kOutput, calls=%fused_computation.3.clone.1 | convolution fusion | flops 137361408 | bytes 5120512 | tf_op jit(solution)/shard_map/while/body/eval_jaxpr/qhpd,khpd->phqk/dot_general | solution.py:73
  158.5 3.3 %fusion.85 = (bf16[2,4,256,512]{2,3,1,0:T(8,128)(2,1)S(1)}, f32[2,4,256]{2,1,0:T(4,128)S(1)}) fusion(f32[2,4,512,256]{3,2,1,0:T(8,128)} %get-tuple-element.404, f32[2,4,256]{2,1,0:T(4,128)S(1)} %select_maximum_fusion.2, pred[256,512]{0,1:T(8,128)(4,1)S(1)} %broadcast_compare_fusion.2), kind=kLoop, calls=%fused_computation.4.clone.1 | loop fusion | flops 6289408 | bytes 6438912 | tf_op jit(solution)/shard_map/while/body/eval_jaxpr/convert_element_type | solution.py:85
  164.0 1.5 fusion.87
  167.5 3.9 %fusion.84 = (f32[2,4,256]{2,1,0:T(4,128)S(1)}, f32[2,4,512,256]{3,2,1,0:T(8,128)}) fusion(pred[256,512]{0,1:T(8,128)(4,1)S(1)} %broadcast_compare_fusion.2, bf16[256,4,2,64]{0,3,1,2:T(8,128)(2,1)S(1)} %get-tuple-element.465, bf16[8,512,4,2,64]{1,4,2,3,0:T(8,128)(2,1)} %get-tuple-element.464, s32[]{:T(128)} %get-tuple-element.448), kind=kOutput, calls=%fused_computation.3.clone.1 | convolution fusion | flops 137361408 | bytes 5120512 | tf_op jit(solution)/shard_map/while/body/eval_jaxpr/qhpd,khpd->phqk/dot_general | solution.py:73
  171.4 3.3 %fusion.85 = (bf16[2,4,256,512]{2,3,1,0:T(8,128)(2,1)S(1)}, f32[2,4,256]{2,1,0:T(4,128)S(1)}) fusion(f32[2,4,512,256]{3,2,1,0:T(8,128)} %get-tuple-element.404, f32[2,4,256]{2,1,0:T(4,128)S(1)} %select_maximum_fusion.2, pred[256,512]{0,1:T(8,128)(4,1)S(1)} %broadcast_compare_fusion.2), kind=kLoop, calls=%fused_computation.4.clone.1 | loop fusion | flops 6289408 | bytes 6438912 | tf_op jit(solution)/shard_map/while/body/eval_jaxpr/convert_element_type | solution.py:85
  176.9 2.7 fusion.87
  181.6 3.9 %fusion.84 = (f32[2,4,256]{2,1,0:T(4,128)S(1)}, f32[2,4,512,256]{3,2,1,0:T(8,128)}) fusion(pred[256,512]{0,1:T(8,128)(4,1)S(1)} %broadcast_compare_fusion.2, bf16[256,4,2,64]{0,3,1,2:T(8,128)(2,1)S(1)} %get-tuple-element.465, bf16[8,512,4,2,64]{1,4,2,3,0:T(8,128)(2,1)} %get-tuple-element.464, s32[]{:T(128)} %get-tuple-element.448), kind=kOutput, calls=%fused_computation.3.clone.1 | convolution fusion | flops 137361408 | bytes 5120512 | tf_op jit(solution)/shard_map/while/body/eval_jaxpr/qhpd,khpd->phqk/dot_general | solution.py:73
  185.5 3.3 %fusion.85 = (bf16[2,4,256,512]{2,3,1,0:T(8,128)(2,1)S(1)}, f32[2,4,256]{2,1,0:T(4,128)S(1)}) fusion(f32[2,4,512,256]{3,2,1,0:T(8,128)} %get-tuple-element.404, f32[2,4,256]{2,1,0:T(4,128)S(1)} %select_maximum_fusion.2, pred[256,512]{0,1:T(8,128)(4,1)S(1)} %broadcast_compare_fusion.2), kind=kLoop, calls=%fused_computation.4.clone.1 | loop fusion | flops 6289408 | bytes 6438912 | tf_op jit(solution)/shard_map/while/body/eval_jaxpr/convert_element_type | solution.py:85
  191.0 2.7 fusion.87
  195.7 3.9 %fusion.84 = (f32[2,4,256]{2,1,0:T(4,128)S(1)}, f32[2,4,512,256]{3,2,1,0:T(8,128)}) fusion(pred[256,512]{0,1:T(8,128)(4,1)S(1)} %broadcast_compare_fusion.2, bf16[256,4,2,64]{0,3,1,2:T(8,128)(2,1)S(1)} %get-tuple-element.465, bf16[8,512,4,2,64]{1,4,2,3,0:T(8,128)(2,1)} %get-tuple-element.464, s32[]{:T(128)} %get-tuple-element.448), kind=kOutput, calls=%fused_computation.3.clone.1 | convolution fusion | flops 137361408 | bytes 5120512 | tf_op jit(solution)/shard_map/while/body/eval_jaxpr/qhpd,khpd->phqk/dot_general | solution.py:73
  199.6 3.3 %fusion.85 = (bf16[2,4,256,512]{2,3,1,0:T(8,128)(2,1)S(1)}, f32[2,4,256]{2,1,0:T(4,128)S(1)}) fusion(f32[2,4,512,256]{3,2,1,0:T(8,128)} %get-tuple-element.404, f32[2,4,256]{2,1,0:T(4,128)S(1)} %select_maximum_fusion.2, pred[256,512]{0,1:T(8,128)(4,1)S(1)} %broadcast_compare_fusion.2), kind=kLoop, calls=%fused_computation.4.clone.1 | loop fusion | flops 6289408 | bytes 6438912 | tf_op jit(solution)/shard_map/while/body/eval_jaxpr/convert_element_type | solution.py:85
  205.1 2.7 fusion.87
  209.8 3.9 %fusion.84 = (f32[2,4,256]{2,1,0:T(4,128)S(1)}, f32[2,4,512,256]{3,2,1,0:T(8,128)}) fusion(pred[256,512]{0,1:T(8,128)(4,1)S(1)} %broadcast_compare_fusion.2, bf16[256,4,2,64]{0,3,1,2:T(8,128)(2,1)S(1)} %get-tuple-element.465, bf16[8,512,4,2,64]{1,4,2,3,0:T(8,128)(2,1)} %get-tuple-element.464, s32[]{:T(128)} %get-tuple-element.448), kind=kOutput, calls=%fused_computation.3.clone.1 | convolution fusion | flops 137361408 | bytes 5120512 | tf_op jit(solution)/shard_map/while/body/eval_jaxpr/qhpd,khpd->phqk/dot_general | solution.py:73
  213.8 3.7 %fusion.85 = (bf16[2,4,256,512]{2,3,1,0:T(8,128)(2,1)S(1)}, f32[2,4,256]{2,1,0:T(4,128)S(1)}) fusion(f32[2,4,512,256]{3,2,1,0:T(8,128)} %get-tuple-element.404, f32[2,4,256]{2,1,0:T(4,128)S(1)} %select_maximum_fusion.2, pred[256,512]{0,1:T(8,128)(4,1)S(1)} %broadcast_compare_fusion.2), kind=kLoop, calls=%fused_computation.4.clone.1 | loop fusion | flops 6289408 | bytes 6438912 | tf_op jit(solution)/shard_map/while/body/eval_jaxpr/convert_element_type | solution.py:85
  219.7 2.7 fusion.87
  224.4 3.9 %fusion.84 = (f32[2,4,256]{2,1,0:T(4,128)S(1)}, f32[2,4,512,256]{3,2,1,0:T(8,128)}) fusion(pred[256,512]{0,1:T(8,128)(4,1)S(1)} %broadcast_compare_fusion.2, bf16[256,4,2,64]{0,3,1,2:T(8,128)(2,1)S(1)} %get-tuple-element.465, bf16[8,512,4,2,64]{1,4,2,3,0:T(8,128)(2,1)} %get-tuple-element.464, s32[]{:T(128)} %get-tuple-element.448), kind=kOutput, calls=%fused_computation.3.clone.1 | convolution fusion | flops 137361408 | bytes 5120512 | tf_op jit(solution)/shard_map/while/body/eval_jaxpr/qhpd,khpd->phqk/dot_general | solution.py:73
  228.3 3.3 %fusion.85 = (bf16[2,4,256,512]{2,3,1,0:T(8,128)(2,1)S(1)}, f32[2,4,256]{2,1,0:T(4,128)S(1)}) fusion(f32[2,4,512,256]{3,2,1,0:T(8,128)} %get-tuple-element.404, f32[2,4,256]{2,1,0:T(4,128)S(1)} %select_maximum_fusion.2, pred[256,512]{0,1:T(8,128)(4,1)S(1)} %broadcast_compare_fusion.2), kind=kLoop, calls=%fused_computation.4.clone.1 | loop fusion | flops 6289408 | bytes 6438912 | tf_op jit(solution)/shard_map/while/body/eval_jaxpr/convert_element_type | solution.py:85
  233.8 2.7 fusion.87
  238.5 3.9 %fusion.84 = (f32[2,4,256]{2,1,0:T(4,128)S(1)}, f32[2,4,512,256]{3,2,1,0:T(8,128)}) fusion(pred[256,512]{0,1:T(8,128)(4,1)S(1)} %broadcast_compare_fusion.2, bf16[256,4,2,64]{0,3,1,2:T(8,128)(2,1)S(1)} %get-tuple-element.465, bf16[8,512,4,2,64]{1,4,2,3,0:T(8,128)(2,1)} %get-tuple-element.464, s32[]{:T(128)} %get-tuple-element.448), kind=kOutput, calls=%fused_computation.3.clone.1 | convolution fusion | flops 137361408 | bytes 5120512 | tf_op jit(solution)/shard_map/while/body/eval_jaxpr/qhpd,khpd->phqk/dot_general | solution.py:73
  242.4 3.3 %fusion.85 = (bf16[2,4,256,512]{2,3,1,0:T(8,128)(2,1)S(1)}, f32[2,4,256]{2,1,0:T(4,128)S(1)}) fusion(f32[2,4,512,256]{3,2,1,0:T(8,128)} %get-tuple-element.404, f32[2,4,256]{2,1,0:T(4,128)S(1)} %select_maximum_fusion.2, pred[256,512]{0,1:T(8,128)(4,1)S(1)} %broadcast_compare_fusion.2), kind=kLoop, calls=%fused_computation.4.clone.1 | loop fusion | flops 6289408 | bytes 6438912 | tf_op jit(solution)/shard_map/while/body/eval_jaxpr/convert_element_type | solution.py:85
  247.9 2.7 fusion.87
  252.6 3.9 %fusion.84 = (f32[2,4,256]{2,1,0:T(4,128)S(1)}, f32[2,4,512,256]{3,2,1,0:T(8,128)}) fusion(pred[256,512]{0,1:T(8,128)(4,1)S(1)} %broadcast_compare_fusion.2, bf16[256,4,2,64]{0,3,1,2:T(8,128)(2,1)S(1)} %get-tuple-element.465, bf16[8,512,4,2,64]{1,4,2,3,0:T(8,128)(2,1)} %get-tuple-element.464, s32[]{:T(128)} %get-tuple-element.448), kind=kOutput, calls=%fused_computation.3.clone.1 | convolution fusion | flops 137361408 | bytes 5120512 | tf_op jit(solution)/shard_map/while/body/eval_jaxpr/qhpd,khpd->phqk/dot_general | solution.py:73
  256.5 3.3 %fusion.85 = (bf16[2,4,256,512]{2,3,1,0:T(8,128)(2,1)S(1)}, f32[2,4,256]{2,1,0:T(4,128)S(1)}) fusion(f32[2,4,512,256]{3,2,1,0:T(8,128)} %get-tuple-element.404, f32[2,4,256]{2,1,0:T(4,128)S(1)} %select_maximum_fusion.2, pred[256,512]{0,1:T(8,128)(4,1)S(1)} %broadcast_compare_fusion.2), kind=kLoop, calls=%fused_computation.4.clone.1 | loop fusion | flops 6289408 | bytes 6438912 | tf_op jit(solution)/shard_map/while/body/eval_jaxpr/convert_element_type | solution.py:85
  262.0 2.7 fusion.87
  264.7 1.5 broadcast_divide_fusion
  270.4 3.4 %all-to-all-start = ((bf16[2,128,512]{1,2,0:T(8,128)(2,1)}), bf16[2,128,512]{1,2,0:T(8,128)(2,1)S(1)}, u32[]{:S(2)}, u32[]{:S(2)}) async-start(bf16[2,128,512]{1,2,0:T(8,128)(2,1)} %copy.59), calls=%async_computation | async-start | bytes 524288 | tf_op jit(solution)/shard_map/all_to_all | solution.py:170
  274.7 5.0 %all-to-all-done = bf16[2,128,512]{1,2,0:T(8,128)(2,1)S(1)} async-done(((bf16[2,128,512]{1,2,0:T(8,128)(2,1)}), bf16[2,128,512]{1,2,0:T(8,128)(2,1)S(1)}, u32[]{:S(2)}, u32[]{:S(2)}) %all-to-all-start) | async-done | bytes 262176 | tf_op jit(solution)/shard_map/all_to_all | solution.py:170
  279.7 3.4 %all-to-all-start.1 = ((bf16[2,128,512]{1,2,0:T(8,128)(2,1)}), bf16[2,128,512]{1,2,0:T(8,128)(2,1)S(1)}, u32[]{:S(2)}, u32[]{:S(2)}) async-start(bf16[2,128,512]{1,2,0:T(8,128)(2,1)} %copy.66), calls=%async_computation.1 | async-start | bytes 524288 | tf_op jit(solution)/shard_map/all_to_all | solution.py:171
  283.1 3.0 fusion.63
  286.1 2.1 all-to-all-done.1
  288.3 3.7 %fusion.19 = bf16[128,2048]{1,0:T(8,128)(2,1)} fusion(f32[128,2048]{1,0:T(8,128)S(1)} %fusion.63, bf16[128,1024]{0,1:T(8,128)(2,1)S(1)} %bitcast.116, bf16[1024,2048]{1,0:T(8,128)(2,1)} %all-gather.16.cloned.1.call-done), kind=kOutput, calls=%fused_computation.29 | convolution fusion | flops 537395200 | bytes 6029312 | tf_op jit(solution)/shard_map/dot_general | solution.py:177
  (353 shorter events, 52.6 us)
Async XLA Ops:
  6.5 42.3 %copy-start = (bf16[4,128,128]{2,1,0:T(8,128)(2,1)S(1)}, bf16[4,128,128]{2,1,0:T(8,128)(2,1)}, u32[]{:S(2)}) copy-start(bf16[4,128,128]{2,1,0:T(8,128)(2,1)} %param.29) | copy-start | bytes 393220
  6.5 6.8 %copy-start.10 = (bf16[2048,512]{1,0:T(8,128)(2,1)S(1)}, bf16[2048,512]{1,0:T(8,128)(2,1)}, u32[]{:S(2)}) copy-start(bf16[2048,512]{1,0:T(8,128)(2,1)} %param.23) | copy-start | bytes 6291460
  6.5 27.6 %all-gather.8.cloned.1.call-start = ((), (), s32[]{:S(2)}) async-start(), calls=%async_computation.2 | async-start | bytes 1572864 | tf_op jit(solution)/shard_map/all_gather | solution.py:159
  10.0 89.4 %all-gather.10.cloned.1.call-start = ((), (), s32[]{:S(2)}) async-start(), calls=%async_computation.3 | async-start | bytes 4456448 | tf_op jit(solution)/shard_map/all_gather | solution.py:58
  10.0 4.9 %copy-start.11 = (bf16[2048,512]{1,0:T(8,128)(2,1)S(1)}, bf16[2048,512]{1,0:T(8,128)(2,1)}, u32[]{:S(2)}) copy-start(bf16[2048,512]{1,0:T(8,128)(2,1)} %param.24) | copy-start | bytes 6291460
  13.3 3.3 %copy-start.12 = (bf16[2048,512]{1,0:T(8,128)(2,1)S(1)}, bf16[2048,512]{1,0:T(8,128)(2,1)}, u32[]{:S(2)}) copy-start(bf16[2048,512]{1,0:T(8,128)(2,1)} %param.25) | copy-start | bytes 6291460
  15.0 3.2 %copy-start.13 = (bf16[2048,512]{1,0:T(8,128)(2,1)S(1)}, bf16[2048,512]{1,0:T(8,128)(2,1)}, u32[]{:S(2)}) copy-start(bf16[2048,512]{1,0:T(8,128)(2,1)} %param.26) | copy-start | bytes 6291460
  16.6 3.1 %copy-start.14 = (bf16[2048,512]{1,0:T(8,128)(2,1)S(1)}, bf16[2048,512]{1,0:T(8,128)(2,1)}, u32[]{:S(2)}) copy-start(bf16[2048,512]{1,0:T(8,128)(2,1)} %param.27) | copy-start | bytes 6291460
  42.5 6.0 %copy-start.15 = (bf16[256,3072]{1,0:T(8,128)(2,1)}, bf16[256,3072]{1,0:T(8,128)(2,1)S(1)}, u32[]{:S(2)}) copy-start(bf16[256,3072]{1,0:T(8,128)(2,1)S(1)} %convolution_convert_fusion) | copy-start | bytes 4718596
  42.5 3.6 %copy-start.20 = (f32[4,512]{1,0:T(4,128)S(1)}, f32[4,512]{1,0:T(4,128)}, u32[]{:S(2)}) copy-start(f32[4,512]{1,0:T(4,128)} %param.28) | copy-start | bytes 24580
  42.5 3.6 %copy-start.21 = (f32[512]{0:T(512)S(1)}, f32[512]{0:T(512)}, u32[]{:S(2)}) copy-start(f32[512]{0:T(512)} %param.31) | copy-start | bytes 6148
  43.5 102.0 %all-gather.12.cloned.1.call-start = ((), (), s32[]{:S(2)}) async-start(), calls=%async_computation.4 | async-start | bytes 4456448 | tf_op jit(solution)/shard_map/all_gather | solution.py:59
  44.3 238.9 %all-gather.14.cloned.1.call-start = ((), (), s32[]{:S(2)}) async-start(), calls=%async_computation.5 | async-start | bytes 6291456 | tf_op jit(solution)/shard_map/all_gather | solution.py:174
  44.8 241.3 %all-gather.16.cloned.1.call-start = ((), (), s32[]{:S(2)}) async-start(), calls=%async_computation.6 | async-start | bytes 6291456 | tf_op jit(solution)/shard_map/all_gather | solution.py:175
  45.4 4.0 %copy-start.22 = (bf16[4,128,128]{2,1,0:T(8,128)(2,1)S(1)}, bf16[4,128,128]{2,1,0:T(8,128)(2,1)}, u32[]{:S(2)}) copy-start(bf16[4,128,128]{2,1,0:T(8,128)(2,1)} %param.30) | copy-start | bytes 393220
  46.1 2.4 collective-permute-start
  55.6 59.9 %copy-start.2 = (f32[256,512]{1,0:T(8,128)}, f32[256,512]{1,0:T(8,128)S(1)}, u32[]{:S(2)}) copy-start(f32[256,512]{1,0:T(8,128)S(1)} %pad.113) | copy-start | bytes 1572868
  56.1 59.4 %copy-start.4 = (f32[256,512]{1,0:T(8,128)}, f32[256,512]{1,0:T(8,128)S(1)}, u32[]{:S(2)}) copy-start(f32[256,512]{1,0:T(8,128)S(1)} %pad.112) | copy-start | bytes 1572868
  80.5 35.0 %copy-start.6 = (f32[256,512]{1,0:T(8,128)}, f32[256,512]{1,0:T(8,128)S(1)}, u32[]{:S(2)}) copy-start(f32[256,512]{1,0:T(8,128)S(1)} %pad.129) | copy-start | bytes 1572868
  80.6 34.9 %copy-start.8 = (f32[256,512]{1,0:T(8,128)}, f32[256,512]{1,0:T(8,128)S(1)}, u32[]{:S(2)}) copy-start(f32[256,512]{1,0:T(8,128)S(1)} %pad.128) | copy-start | bytes 1572868
  99.4 16.2 %copy-start.18 = (f32[512]{0:T(512)}, f32[512]{0:T(512)S(1)}, u32[]{:S(2)}) copy-start(f32[512]{0:T(512)S(1)} %get-tuple-element.149) | copy-start | bytes 6148
  161.8 0.6 copy-start.16
  164.0 1.5 copy-start.17
  174.7 0.6 copy-start.16
  176.9 2.7 copy-start.17
  188.8 0.6 copy-start.16
  191.0 2.7 copy-start.17
  202.9 0.6 copy-start.16
  205.1 2.7 copy-start.17
  217.5 0.6 copy-start.16
  219.6 2.7 copy-start.17
  231.6 0.6 copy-start.16
  233.7 2.7 copy-start.17
  245.7 0.6 copy-start.16
  247.9 2.7 copy-start.17
  259.8 0.6 copy-start.16
  262.0 2.7 copy-start.17
  264.7 3.4 %copy-start.3 = (f32[256,512]{1,0:T(8,128)S(1)}, f32[256,512]{1,0:T(8,128)}, u32[]{:S(2)}) copy-start(f32[256,512]{1,0:T(8,128)} %copy-done.2) | copy-start | bytes 1572868
  264.7 3.4 %copy-start.5 = (f32[256,512]{1,0:T(8,128)S(1)}, f32[256,512]{1,0:T(8,128)}, u32[]{:S(2)}) copy-start(f32[256,512]{1,0:T(8,128)} %copy-done.4) | copy-start | bytes 1572868
  264.7 3.4 %copy-start.7 = (f32[256,512]{1,0:T(8,128)S(1)}, f32[256,512]{1,0:T(8,128)}, u32[]{:S(2)}) copy-start(f32[256,512]{1,0:T(8,128)} %copy-done.6) | copy-start | bytes 1572868
  264.7 3.4 %copy-start.9 = (f32[256,512]{1,0:T(8,128)S(1)}, f32[256,512]{1,0:T(8,128)}, u32[]{:S(2)}) copy-start(f32[256,512]{1,0:T(8,128)} %copy-done.8) | copy-start | bytes 1572868
  264.7 3.4 %copy-start.19 = (f32[512]{0:T(512)S(1)}, f32[512]{0:T(512)}, u32[]{:S(2)}) copy-start(f32[512]{0:T(512)} %copy-done.18) | copy-start | bytes 6148
  270.4 9.3 %all-to-all-start = ((bf16[2,128,512]{1,2,0:T(8,128)(2,1)}), bf16[2,128,512]{1,2,0:T(8,128)(2,1)S(1)}, u32[]{:S(2)}, u32[]{:S(2)}) async-start(bf16[2,128,512]{1,2,0:T(8,128)(2,1)} %copy.59), calls=%async_computation | async-start | bytes 524288 | tf_op jit(solution)/shard_map/all_to_all | solution.py:170
  279.7 8.6 %all-to-all-start.1 = ((bf16[2,128,512]{1,2,0:T(8,128)(2,1)}), bf16[2,128,512]{1,2,0:T(8,128)(2,1)S(1)}, u32[]{:S(2)}, u32[]{:S(2)}) async-start(bf16[2,128,512]{1,2,0:T(8,128)(2,1)} %copy.66), calls=%async_computation.1 | async-start | bytes 524288 | tf_op jit(solution)/shard_map/all_to_all | solution.py:171
  283.1 8.9 %copy-start.1 = (bf16[4,128,128]{2,1,0:T(8,128)(2,1)S(1)}, bf16[4,128,128]{2,1,0:T(8,128)(2,1)}, u32[]{:S(2)}) copy-start(bf16[4,128,128]{2,1,0:T(8,128)(2,1)} %param.29) | copy-start | bytes 393220
Sparse Core Ops, SparseCore 0:
  10.1 23.9 all-gather.7
  43.6 50.6 all-gather.9
  96.5 48.9 all-gather.11
  146.9 55.2 all-gather.13
  203.6 56.7 all-gather.15
where the time goes:
time: 301 us; the launch traced here: 299 us
  local copies, waits for them, and re-layouts  89.6 us (30%)
  matrix products  67.2 us (22%)
  other arithmetic  43.6 us (14%)
  blocking collectives  42.2 us (14%)
  waiting for transfers between devices  32 us (11%)
  between operations  14.3 us (5%)
  starting transfers between devices  8.62 us (3%)
    all_gather x2, blocking collectives, carried_in(): pieces = jax.tree.map(lambda part: lax.all_gather(part, axis), value)  42.2 us
    dot_general x8, matrix products, one_block(): jnp.einsum('qhpd,khpd->phqk', query_heads, key_block, preferred_element_t...  31.2 us
    unnamed x51, local copies, waits for them, and re-layouts  30 us
    convert_element_type x8, other arithmetic, one_block(): raised.astype(jnp.bfloat16)  26.7 us
    dynamic_slice x24, local copies, waits for them, and re-layouts, attention(): lax.scan(one_block, running, (key_blocks, value_blocks, block_starts))  22.5 us
    dot_general x8, matrix products, one_block(): jnp.einsum('phqk,khe->phqe', raised.astype(jnp.bfloat16), value_block, pr...  20.3 us
    reshape x1, local copies, waits for them, and re-layouts, attention(): key_piece.reshape(block_count, block_len, local_heads, 2, head_dim)  16.1 us
    all_gather x1, waiting for transfers between devices, body(): lax.all_gather(normed, 'tp', axis=0, tiled=True)  12.8 us
  transfers between devices with their start and end apart: 8, of which 5 were waited for; matrix products, arithmetic and copies ran while one was open for 60% of the time, Pallas kernels for 0%

commit v1 on v0

v1 whole, which is shorter than its diff:
```python
import functools

import jax
import jax.numpy as jnp
from jax import lax
from jax.experimental import pallas as pl
from jax.experimental.pallas import tpu as pltpu
from jax.sharding import PartitionSpec as P

EPS_INPUT = 1e-06
EPS_HEAD = 1e-05
RATE_SCALE = 8.0
HEAD_FACTOR = 0.8
MASKED = -1e30


def passed_along(block, axis, distance):
    devices = range(lax.axis_size(axis))
    route = [(i - distance, i) for i in devices if i - distance in devices]
    return lax.ppermute(block, axis, route)


def rms_rows(values, gain, epsilon):
    mean_square = jnp.mean(values * values, axis=-1, keepdims=True)
    return values * lax.rsqrt(mean_square + epsilon) * gain


def attn_kernel(plane, idx_ref, lam_ref, q_ref, kv_ref, gain_ref, o_ref, m_ref, l_ref, acc_ref):
    rows = q_ref.shape[1]
    width = q_ref.shape[2]
    half = width // 2
    mine = pl.program_id(0) * plane + idx_ref[0]
    q = q_ref[0].astype(jnp.float32) * (half ** (-0.5))
    lane = lax.broadcasted_iota(jnp.int32, q.shape, 1)
    both = jnp.concatenate(
        [jnp.where(lane < half, q, 0.0), jnp.where(lane >= half, q, 0.0)], axis=0
    ).astype(jnp.bfloat16)
    m_ref[...] = jnp.full(m_ref.shape, MASKED, jnp.float32)
    l_ref[...] = jnp.zeros(l_ref.shape, jnp.float32)
    acc_ref[...] = jnp.zeros(acc_ref.shape, jnp.float32)

    def step(pair, masked):
        first = 2 * pair
        r, z = lax.rem(first, plane), lax.div(first, plane)
        keys = jnp.concatenate([kv_ref[r, z, :, :width], kv_ref[r + 1, z, :, :width]], axis=0)
        vals = jnp.concatenate([kv_ref[r, z, :, width:], kv_ref[r + 1, z, :, width:]], axis=0)
        s = lax.dot_general(
            both, keys, (((1,), (1,)), ((), ())), preferred_element_type=jnp.float32
        )
        if masked:
            qpos = lax.rem(lax.broadcasted_iota(jnp.int32, s.shape, 0), rows) + mine * rows
            kpos = lax.broadcasted_iota(jnp.int32, s.shape, 1) + first * rows
            s = jnp.where(kpos <= qpos, s, MASKED)
        old = m_ref[...]
        new = jnp.maximum(old, jnp.max(s, axis=-1, keepdims=True))
        factor = jnp.exp(old - new)
        p = jnp.exp(s - new[:, :1])
        m_ref[...] = new
        part = p[:, :128]
        for c in range(1, s.shape[1] // 128):
            part = part + p[:, c * 128 : (c + 1) * 128]
        l_ref[...] = l_ref[...] * factor + part
        acc_ref[...] = acc_ref[...] * factor + jnp.dot(
            p.astype(jnp.bfloat16), vals, preferred_element_type=jnp.float32
        )

    def body(pair, _):
        step(pair, False)
        return 0

    last = lax.div(mine, 2)
    lax.fori_loop(0, last, body, 0)
    step(last, True)
    total = jnp.sum(l_ref[...], axis=-1, keepdims=True)
    out = acc_ref[...] / total
    per_head = out[:rows] - lam_ref[0] * out[rows:]
    o_ref[0] = (rms_rows(per_head, gain_ref[...], EPS_HEAD) * HEAD_FACTOR).astype(o_ref.dtype)


def attention(queries, keys, values, head_lambda, head_gain):
    rows = queries.shape[0]
    heads = head_lambda.shape[0]
    sp = lax.axis_size("sp")
    plane = sp // heads
    strided = [[r + plane * g for g in range(heads)] for r in range(plane)]
    planes = [[r + plane * g for r in range(plane)] for g in range(heads)]
    width = queries.shape[1] // heads
    vdim = values.shape[1] // heads
    packed = jnp.concatenate(
        [part.reshape(rows, heads, -1).swapaxes(0, 1) for part in (queries, keys, values)], axis=2
    )
    mixed = lax.all_to_all(
        packed, "sp", split_axis=0, concat_axis=0, tiled=True, axis_index_groups=strided
    )
    kv = lax.all_gather(mixed[:, :, width:], "sp", axis=0, axis_index_groups=planes)
    index = lax.axis_index("sp")
    head = index // plane
    lam = lax.dynamic_slice_in_dim(head_lambda, head, 1)
    gain = lax.dynamic_slice_in_dim(head_gain.reshape(heads, vdim), head, 1, 0)
    out = pl.pallas_call(
        functools.partial(attn_kernel, plane),
        grid=(heads,),
        out_shape=jax.ShapeDtypeStruct((heads, rows, vdim), jnp.bfloat16),
        in_specs=[
            pl.BlockSpec(memory_space=pltpu.SMEM),
            pl.BlockSpec(memory_space=pltpu.SMEM),
            pl.BlockSpec((1, rows, width), lambda g: (g, 0, 0)),
            pl.BlockSpec(memory_space=pltpu.VMEM),
            pl.BlockSpec(memory_space=pltpu.VMEM),
        ],
        out_specs=pl.BlockSpec((1, rows, vdim), lambda g: (g, 0, 0)),
        scratch_shapes=[
            pltpu.VMEM((2 * rows, 128), jnp.float32),
            pltpu.VMEM((2 * rows, 128), jnp.float32),
            pltpu.VMEM((2 * rows, vdim), jnp.float32),
        ],
        name="attn",
    )((index % plane).astype(jnp.int32).reshape(1), lam, mixed[:, :, :width], kv, gain)
    back = lax.all_to_all(
        out, "sp", split_axis=0, concat_axis=0, tiled=True, axis_index_groups=strided
    )
    return back.swapaxes(0, 1).reshape(rows, heads * vdim)


def scan_kernel(idx_ref, rec_ref, early_ref, taps_ref, gr_ref, gi_ref, rate_ref, p_ref, s_ref):
    rows, width = rec_ref.shape
    taps = taps_ref.shape[0]
    at = lax.broadcasted_iota(jnp.int32, (rows, width), 0)
    x = rec_ref[...].astype(jnp.float32)
    early = early_ref[...].astype(jnp.float32)
    conv = jnp.zeros((rows, width), jnp.float32)
    for offset in range(taps):
        back = taps - 1 - offset
        if back:
            moved = pltpu.roll(x, back, 0)
            for row in range(back):
                moved = jnp.where(at == row, early[taps - 1 - back + row][None], moved)
        else:
            moved = x
        conv = conv + moved * taps_ref[offset][None]
    conv16 = conv.astype(jnp.bfloat16)
    size = gr_ref.shape[1]
    gates, flows = [], []
    for n in range(gr_ref.shape[0]):
        piece = conv16[:, n * size : (n + 1) * size]
        gates.append(jnp.dot(piece, gr_ref[n], preferred_element_type=jnp.float32))
        flows.append(jnp.dot(piece, gi_ref[n], preferred_element_type=jnp.float32))
    recur = jax.nn.sigmoid(jnp.concatenate(gates, axis=1))
    inflow = jax.nn.sigmoid(jnp.concatenate(flows, axis=1))
    log_decay = -RATE_SCALE * recur * rate_ref[...]
    a = jnp.exp(log_decay)
    y = 2.0 * log_decay
    small = -y * (1.0 + y * (1 / 2) * (1.0 + y * (1 / 3) * (1.0 + y * (1 / 4) * (1.0 + y * (1 / 5) * (1.0 + y * (1 / 6))))))
    fall = jnp.where(y > -0.35, small, 1.0 - jnp.exp(y))
    norm_in = jnp.where((at == 0) & (idx_ref[0] == 0), 1.0, jnp.sqrt(fall))
    b = norm_in * inflow * conv16.astype(jnp.float32)
    shift = 1
    while shift < rows:
        keep = at >= shift
        pa = jnp.where(keep, pltpu.roll(a, shift, 0), 1.0)
        pb = jnp.where(keep, pltpu.roll(b, shift, 0), 0.0)
        b = b + a * pb
        a = a * pa
        shift *= 2
    p_ref[...] = a
    s_ref[...] = b


def recurrence(rec_in, rec_gate, conv_taps, gate_recur, gate_input, decay_rate):
    rows, width = rec_in.shape
    taps = conv_taps.shape[0]
    early = passed_along(rec_in[rows - (taps - 1) :], "sp", 1)
    mine = lax.axis_index("sp")
    products, partial_states = pl.pallas_call(
        scan_kernel,
        out_shape=[jax.ShapeDtypeStruct((rows, width), jnp.float32)] * 2,
        in_specs=[pl.BlockSpec(memory_space=pltpu.SMEM)]
        + [pl.BlockSpec(memory_space=pltpu.VMEM)] * 6,
        out_specs=[pl.BlockSpec(memory_space=pltpu.VMEM)] * 2,
        name="scan",
    )(
        mine.astype(jnp.int32).reshape(1),
        rec_in,
        early,
        conv_taps,
        gate_recur,
        gate_input,
        decay_rate.reshape(1, width),
    )
    ends = jnp.concatenate([products[rows - 1 :], partial_states[rows - 1 :]], axis=0)
    pieces = lax.all_gather(ends, "sp")
    carry = jnp.zeros((width,), jnp.float32)
    for position in range(lax.axis_size("sp") - 1):
        longer = pieces[position, 0] * carry + pieces[position, 1]
        carry = jnp.where(position < mine, longer, carry)
    states = partial_states + products * carry[None, :]
    return (states * jax.nn.silu(rec_gate.astype(jnp.float32))).astype(jnp.bfloat16)


def body(
    tokens,
    norm_gain,
    w_query,
    w_key,
    w_value,
    w_att_gate,
    w_rec_in,
    w_rec_gate,
    conv_taps,
    gate_recur,
    gate_input,
    decay_rate,
    head_lambda,
    head_gain,
    out_att,
    out_rec,
):
    tp = lax.axis_size("tp")
    normed = rms_rows(tokens.astype(jnp.float32), norm_gain, EPS_INPUT).astype(jnp.bfloat16)
    whole = lax.all_gather(normed, "tp", axis=0, tiled=True)
    queries, keys, values, att_gate, rec_in, rec_gate = [
        jnp.dot(whole, weight, preferred_element_type=jnp.float32).astype(jnp.bfloat16)
        for weight in (w_query, w_key, w_value, w_att_gate, w_rec_in, w_rec_gate)
    ]
    head_out = attention(queries, keys, values, head_lambda, head_gain)
    att_mixed = (
        head_out.astype(jnp.float32) * jax.nn.silu(att_gate.astype(jnp.float32))
    ).astype(jnp.bfloat16)
    rec_mixed = recurrence(rec_in, rec_gate, conv_taps, gate_recur, gate_input, decay_rate)
    partial = jnp.dot(att_mixed, out_att, preferred_element_type=jnp.float32) + jnp.dot(
        rec_mixed, out_rec, preferred_element_type=jnp.float32
    )
    partial = partial.astype(jnp.bfloat16).reshape(tp, -1, partial.shape[1])
    parts = lax.all_to_all(partial, "tp", split_axis=0, concat_axis=0, tiled=True)
    return jnp.sum(parts.astype(jnp.float32), axis=0).astype(jnp.bfloat16)


def solution(mesh):
    return jax.shard_map(
        body,
        mesh=mesh,
        in_specs=(
            P(("sp", "tp"), None),
            P(),
            P(None, "tp"),
            P(None, "tp"),
            P(None, "tp"),
            P(None, "tp"),
            P(None, "tp"),
            P(None, "tp"),
            P(None, "tp"),
            P("tp", None, None),
            P("tp", None, None),
            P("tp"),
            P("tp"),
            P("tp"),
            P("tp", None),
            P("tp", None),
        ),
        out_specs=P(("sp", "tp"), None),
        check_vma=False,
    )
```

time: 301 us -> 168 us (0.56)
  local copies, waits for them, and re-layouts: 89.6 us -> 6.31 us
  matrix products: 67.2 us -> 20.8 us
  other arithmetic: 43.6 us -> 4.75 us
  Pallas kernels: 0 us -> 21.6 us
  blocking collectives: 42.2 us -> 62.1 us
  starting transfers between devices: 8.62 us -> 4.74 us
    dot_general x21 -> x6, matrix products: 67.2 us -> 20.8 us  [the longest x4 10.5 us: body(): jnp.dot(whole, weight, preferred_element_type=jnp.float32)]
    all_to_all x0 -> x2, blocking collectives: none -> 40.5 us  [the longest x1 24.3 us: attention(): lax.all_to_all(packed, 'sp', split_axis=0, concat_axis=0, tiled=True, axi...]
    unnamed x51 -> x12, local copies, waits for them, and re-layouts: 30 us -> 0.61 us
    convert_element_type x10 -> x0, other arithmetic: 28.2 us -> none  [the longest x8 26.7 us: one_block(): raised.astype(jnp.bfloat16)]
    reshape x3, local copies, waits for them, and re-layouts: 23.3 us -> 0.51 us  [attention(): part.reshape(rows, heads, -1).swapaxes(0, 1)]
    pallas_call x0 -> x2, Pallas kernels: none -> 21.6 us  [the longest x1 17.8 us: attention(): pl.pallas_call(functools.partial(attn_kernel, plane), grid=(heads,), out_...]
    dynamic_slice x39 -> x2, local copies, waits for them, and re-layouts: 22.7 us -> 1.75 us  [the longest x1 1.18 us: attention(): gain = lax.dynamic_slice_in_dim(head_gain.reshape(heads, vdim), head, 1, 0)]
    all_gather x2 -> x1, blocking collectives: 42.2 us -> 21.6 us  [recurrence(): pieces = lax.all_gather(ends, 'sp')]
  transfers between devices with their start and end apart: 8 -> 4, of which waited for: 5 -> 2; matrix products, arithmetic and copies ran while one was open for 60% -> 4% of each run, Pallas kernels for 0% -> 2%
where the time goes in v1:
time: 168 us; the launch traced here: 167 us
  blocking collectives  62.1 us (37%)
  waiting for transfers between devices  33.7 us (20%)
  Pallas kernels  21.6 us (13%)
  matrix products  20.8 us (12%)
  between operations  13.6 us (8%)
  local copies, waits for them, and re-layouts  6.31 us (4%)
  other arithmetic  4.75 us (3%)
  starting transfers between devices  4.74 us (3%)
    all_to_all x1, blocking collectives, attention(): lax.all_to_all(packed, 'sp', split_axis=0, concat_axis=0, tiled=True, axi...  24.3 us
    all_gather x1, waiting for transfers between devices, body(): whole = lax.all_gather(normed, 'tp', axis=0, tiled=True)  24.1 us
    all_gather x1, blocking collectives, recurrence(): pieces = lax.all_gather(ends, 'sp')  21.6 us
    pallas_call x1, Pallas kernels, attention(): pl.pallas_call(functools.partial(attn_kernel, plane), grid=(heads,), out_...  17.8 us
    all_to_all x1, blocking collectives, body(): lax.all_to_all(partial, 'tp', split_axis=0, concat_axis=0, tiled=True)  16.2 us
    dot_general x4, matrix products, body(): jnp.dot(whole, weight, preferred_element_type=jnp.float32)  10.5 us
    all_to_all x1, waiting for transfers between devices, attention(): lax.all_to_all(out, 'sp', split_axis=0, concat_axis=0, tiled=True, axis_i...  9.51 us
    dot_general x1, matrix products, body(): jnp.dot(rec_mixed, out_rec, preferred_element_type=jnp.float32)  5.59 us
  transfers between devices with their start and end apart: 4, of which 2 were waited for; matrix products, arithmetic and copies ran while one was open for 4% of the time, Pallas kernels for 2%

profile of v1, /device:TPU:0, one launch (start us, length us, event | category | flops | bytes accessed | tf_op | source)
XLA Modules:
  0.0 167.5 jit_solution(10999584766733727252)
XLA Ops:
  6.5 0.0 copy-start
  6.5 0.0 all-gather.6.cloned.1.call-start
  6.5 1.4 fusion.3
  7.9 2.0 %fusion.5 = bf16[128,2048]{1,0:T(8,128)(2,1)} fusion(bf16[128,2048]{1,0:T(8,128)(2,1)} %param.16, f32[2048]{0:T(1024)} %param.17, f32[128]{0:T(128)S(1)} %add_rsqrt_fusion), kind=kLoop, calls=%fused_computation.14 | loop fusion | flops 1048576 | bytes 1057280 | tf_op jit(solution)/shard_map/convert_element_type | solution.py:219
  10.0 0.0 all-gather.6.cloned.1.call-update
  10.0 0.0 all-gather.8.cloned.1.call-start
  10.0 24.1 %all-gather.6.cloned.1.call-done = bf16[256,2048]{1,0:T(8,128)(2,1)} async-done(((bf16[128,2048]{1,0:T(8,128)(2,1)}), bf16[256,2048]{1,0:T(8,128)(2,1)}) %all-gather.6.cloned.1.call-update) | async-done | bytes 1048592 | tf_op jit(solution)/shard_map/all_gather | solution.py:220
  34.1 2.6 %convolution_convert_fusion.3 = bf16[256,512]{1,0:T(8,128)(2,1)S(1)} fusion(bf16[256,2048]{1,0:T(8,128)(2,1)} %all-gather.6.cloned.1.call-done, bf16[2048,512]{1,0:T(8,128)(2,1)} %param.20), kind=kOutput, calls=%fused_computation.7 | convolution fusion | flops 537001984 | bytes 3407872 | tf_op jit(solution)/shard_map/dot_general | solution.py:222
  36.8 0.1 copy.29
  36.9 0.2 copy.30
  37.1 2.6 %convolution_convert_fusion.4 = bf16[256,512]{1,0:T(8,128)(2,1)S(1)} fusion(bf16[256,2048]{1,0:T(8,128)(2,1)} %all-gather.6.cloned.1.call-done, bf16[2048,512]{1,0:T(8,128)(2,1)} %param.19), kind=kOutput, calls=%fused_computation.8 | convolution fusion | flops 537001984 | bytes 3407872 | tf_op jit(solution)/shard_map/dot_general | solution.py:222
  39.7 0.1 copy.27
  39.9 0.2 copy.28
  40.0 2.6 %convolution_convert_fusion.5 = bf16[256,512]{1,0:T(8,128)(2,1)S(1)} fusion(bf16[256,2048]{1,0:T(8,128)(2,1)} %all-gather.6.cloned.1.call-done, bf16[2048,512]{1,0:T(8,128)(2,1)} %param.18), kind=kOutput, calls=%fused_computation.9 | convolution fusion | flops 537001984 | bytes 3407872 | tf_op jit(solution)/shard_map/dot_general | solution.py:222
  42.7 0.1 copy.25
  42.8 0.2 copy.26
  43.0 0.1 pad_maximum_fusion
  43.1 24.3 %all_to_all.15 = bf16[4,256,384]{2,1,0:T(8,128)(2,1)S(1)} all-to-all(bf16[4,256,384]{2,1,0:T(8,128)(2,1)S(1)} %pad_maximum_fusion), channel_id=1, replica_groups={{0,8,16,24},{2,10,18,26},{4,12,20,28},{6,14,22,30},{1,9,17,25},{3,11,19..., dimensions={0} | all-to-all | bytes 1572864 | tf_op jit(solution)/shard_map/all_to_all | solution.py:92
  67.4 0.8 slice.141
  68.3 0.0 copy-start.5
  68.3 0.0 all-gather.8.cloned.1.call-update
  68.3 2.6 %convolution_convert_fusion.1.rec_ref = bf16[256,512]{1,0:T(8,128)(2,1)S(1)} fusion(bf16[256,2048]{1,0:T(8,128)(2,1)} %all-gather.6.cloned.1.call-done, bf16[2048,512]{1,0:T(8,128)(2,1)} %param.22), kind=kOutput, calls=%fused_computation.5 | convolution fusion | flops 537001984 | bytes 3407872 | tf_op jit(solution)/shard_map/dot_general | solution.py:222
  70.9 0.0 copy-start.1
  71.0 1.3 collective-permute-start
  72.3 1.2 constant_dynamic-slice_fusion.gain_ref
  73.4 0.0 copy-done.5
  73.4 0.6 dynamic_slice.6.lam_ref
  74.0 0.0 collective-permute-done.early_ref
  74.0 0.0 copy-done.1
  74.0 0.6 copy-done.2
  74.6 3.8 %scan.1 = (f32[256,512]{1,0:T(8,128)}, f32[256,512]{1,0:T(8,128)}) custom-call(s32[1]{0:T(128)} %bitcast.10.idx_ref, bf16[256,512]{1,0:T(8,128)(2,1)} %copy-done.1, bf16[3,512]{1,0:T(4,128)(2,1)} %copy-done.2, f32[4,512]{1,0:T(4,128)} %taps_ref.1, bf16[4,128,128]{2,1,0:T(8,128)(2,1)} %gr_ref.1, bf16[4,128,128]{2,1,0:T(8,128)(2,1)} %gi_ref.1, f32[1,512]{1,0:T(1,128)} %bitcast.105), custom_call_target="tpu_custom_call" | custom-call | tf_op jit(solution)/shard_map/scan/pallas_call | solution.py:174
  78.4 0.7 slice.109
  79.1 0.7 slice.108
  79.9 21.6 %all-gather.2 = f32[16,2,512]{2,1,0:T(2,128)S(1)} all-gather(f32[1,2,512]{2,1,0:T(2,128)S(1)} %maximum_bitcast_fusion), channel_id=3, replica_groups=mesh['sp'=16,'tp'=2] {'sp'}, dimensions={0}, use_global_device_ids=true | all-gather | bytes 69632 | tf_op jit(solution)/shard_map/all_gather | solution.py:191
  101.5 0.7 slice.140.q_ref
  102.2 17.8 %attn.1 = bf16[4,256,128]{2,1,0:T(8,128)(2,1)} custom-call(s32[1]{0:T(128)} %bitcast.idx_ref, f32[1]{0:T(128)} %dynamic_slice.6.lam_ref, bf16[4,256,128]{2,1,0:T(8,128)(2,1)} %slice.140.q_ref, bf16[4,4,256,256]{3,2,1,0:T(8,128)(2,1)} %bitcast.68, f32[1,128]{1,0:T(1,128)} %constant_dynamic-slice_fusion.gain_ref), custom_call_target="tpu_custom_call" | custom-call | tf_op jit(solution)/shard_map/attn/pallas_call | solution.py:100
  120.0 3.4 %all-to-all-start.1 = ((bf16[4,256,128]{2,1,0:T(8,128)(2,1)}), bf16[4,256,128]{2,1,0:T(8,128)(2,1)S(1)}, u32[]{:S(2)}, u32[]{:S(2)}) async-start(bf16[4,256,128]{2,1,0:T(8,128)(2,1)} %attn.1), calls=%async_computation.1 | async-start | bytes 524288 | tf_op jit(solution)/shard_map/all_to_all | solution.py:119
  123.5 0.1 add_select_fusion
  123.5 0.0 copy-start.3
  123.5 0.0 copy-start.4
  123.6 9.5 %all-to-all-done.1 = bf16[4,256,128]{2,1,0:T(8,128)(2,1)S(1)} async-done(((bf16[4,256,128]{2,1,0:T(8,128)(2,1)}), bf16[4,256,128]{2,1,0:T(8,128)(2,1)S(1)}, u32[]{:S(2)}, u32[]{:S(2)}) %all-to-all-start.1) | async-done | bytes 262176 | tf_op jit(solution)/shard_map/all_to_all | solution.py:119
  133.1 0.0 copy-done
  133.1 4.7 %fusion.7 = f32[256,2048]{1,0:T(8,128)} fusion(bf16[512,2048]{1,0:T(8,128)(2,1)S(1)} %copy-done, bf16[256,2048]{1,0:T(8,128)(2,1)} %all-gather.6.cloned.1.call-done, bf16[2048,512]{1,0:T(8,128)(2,1)} %param.21, bf16[4,256,128]{2,1,0:T(8,128)(2,1)S(1)} %all-to-all-done.1), kind=kOutput, calls=%fused_computation.20 | convolution fusion | flops 1074921472 | bytes 7602176 | tf_op jit(solution)/shard_map/dot_general | solution.py:230
  137.7 0.0 copy-done.3
  137.7 0.0 copy-done.4
  137.7 5.6 %fusion = bf16[256,2048]{1,0:T(8,128)(2,1)} fusion(f32[256,2048]{1,0:T(8,128)} %fusion.7, bf16[512,2048]{1,0:T(8,128)(2,1)} %param.31, f32[256,512]{1,0:T(8,128)S(1)} %copy-done.4, f32[256,512]{1,0:T(8,128)S(1)} %copy-done.3, bf16[256,2048]{1,0:T(8,128)(2,1)} %all-gather.6.cloned.1.call-done, bf16[2048,512]{1,0:T(8,128)(2,1)} %param.23, ...), kind=kOutput, calls=%fused_computation.1 | convolution fusion | flops 1076101120 | bytes 9439232 | tf_op jit(solution)/shard_map/dot_general | solution.py:230
  143.3 16.2 %all_to_all.16 = bf16[2,128,2048]{2,1,0:T(8,128)(2,1)S(1)} all-to-all(bf16[2,128,2048]{2,1,0:T(8,128)(2,1)} %bitcast.69), channel_id=1, replica_groups=mesh['sp'=16,'tp'=2] {'tp'}, dimensions={0} | all-to-all | bytes 2097152 | tf_op jit(solution)/shard_map/all_to_all | solution.py:234
  159.5 1.1 reduce_sum.22
  (7 shorter events, 0.1 us)
Async XLA Ops:
  6.5 126.5 %copy-start = (bf16[512,2048]{1,0:T(8,128)(2,1)S(1)}, bf16[512,2048]{1,0:T(8,128)(2,1)}, u32[]{:S(2)}) copy-start(bf16[512,2048]{1,0:T(8,128)(2,1)} %param.30) | copy-start | bytes 6291460
  6.5 27.6 %all-gather.6.cloned.1.call-start = ((), (), s32[]{:S(2)}) async-start(), calls=%async_computation.3 | async-start | bytes 1572864 | tf_op jit(solution)/shard_map/all_gather | solution.py:220
  10.0 92.2 %all-gather.8.cloned.1.call-start = ((), (), s32[]{:S(2)}) async-start(), calls=%async_computation.4 | async-start | bytes 2621440 | tf_op jit(solution)/shard_map/all_gather | solution.py:95
  68.3 5.2 %copy-start.5 = (f32[4]{0:T(128)S(1)}, f32[4]{0:T(128)}, u32[]{:S(2)}) copy-start(f32[4]{0:T(128)} %param.28) | copy-start | bytes 52
  70.9 3.1 %copy-start.1 = (bf16[256,512]{1,0:T(8,128)(2,1)}, bf16[256,512]{1,0:T(8,128)(2,1)S(1)}, u32[]{:S(2)}) copy-start(bf16[256,512]{1,0:T(8,128)(2,1)S(1)} %convolution_convert_fusion.1.rec_ref) | copy-start | bytes 786436
  71.0 3.1 %collective-permute-start = (bf16[3,512]{1,0:T(4,128)(2,1)S(1)}, bf16[3,512]{1,0:T(4,128)(2,1)S(1)}, u32[]{:S(2)}, u32[]{:S(2)}) collective-permute-start(bf16[3,512]{1,0:T(4,128)(2,1)S(1)} %slice.142), channel_id=1, source_target_pairs={{0,2},{2,4},{4,6},{6,8},{8,10},{10,12},{12,14},{14,16},{16,18},{18... | collective-permute-start | bytes 9224 | tf_op jit(solution)/shard_map/ppermute | solution.py:20
  74.0 0.6 copy-start.2
  120.0 13.0 %all-to-all-start.1 = ((bf16[4,256,128]{2,1,0:T(8,128)(2,1)}), bf16[4,256,128]{2,1,0:T(8,128)(2,1)S(1)}, u32[]{:S(2)}, u32[]{:S(2)}) async-start(bf16[4,256,128]{2,1,0:T(8,128)(2,1)} %attn.1), calls=%async_computation.1 | async-start | bytes 524288 | tf_op jit(solution)/shard_map/all_to_all | solution.py:119
  123.5 14.2 %copy-start.3 = (f32[256,512]{1,0:T(8,128)S(1)}, f32[256,512]{1,0:T(8,128)}, u32[]{:S(2)}) copy-start(f32[256,512]{1,0:T(8,128)} %get-tuple-element.8) | copy-start | bytes 1572868
  123.5 14.2 %copy-start.4 = (f32[256,512]{1,0:T(8,128)S(1)}, f32[256,512]{1,0:T(8,128)}, u32[]{:S(2)}) copy-start(f32[256,512]{1,0:T(8,128)} %get-tuple-element.7) | copy-start | bytes 1572868
Sparse Core Ops, SparseCore 0:
  10.1 23.9 all-gather.5
  68.4 20.8 all-gather.7

commit v2 on v0

v2 whole, which is shorter than its diff:
```python
import functools

import jax
import jax.numpy as jnp
from jax import lax
from jax.experimental import pallas as pl
from jax.experimental.pallas import tpu as pltpu
from jax.sharding import PartitionSpec as P

EPS_INPUT = 1e-06
EPS_HEAD = 1e-05
RATE_SCALE = 8.0
HEAD_FACTOR = 0.8
MASKED = -1e30
MESH = pl.DeviceIdType.MESH
VMEM = pl.BlockSpec(memory_space=pltpu.VMEM)
ANY = pl.BlockSpec(memory_space=pl.ANY)
SMEM = pl.BlockSpec(memory_space=pltpu.SMEM)
LIMIT = 60 * 1024 * 1024


def rms_rows(values, gain, epsilon):
    mean_square = jnp.mean(values * values, axis=-1, keepdims=True)
    return values * lax.rsqrt(mean_square + epsilon) * gain


def greet(axis, size):
    barrier = pltpu.get_barrier_semaphore()
    me = lax.axis_index(axis)

    def one(k, _):
        pl.semaphore_signal(
            barrier, inc=1, device_id={axis: lax.rem(me + k, size)}, device_id_type=MESH
        )
        return 0

    lax.fori_loop(1, size, one, 0)


def remote(src, dst, send, recv, device):
    return pltpu.make_async_remote_copy(
        src_ref=src, dst_ref=dst, send_sem=send, recv_sem=recv, device_id=device, device_id_type=MESH
    )


def fall_of(y):
    series = 1.0 + y * (1 / 6)
    for n in (5, 4, 3, 2):
        series = 1.0 + y * (1 / n) * series
    return jnp.where(y > -0.35, -y * series, 1.0 - jnp.exp(y))


def front_kernel(
    tp,
    sp,
    heads,
    tok_ref,
    ngain_ref,
    wq,
    wk,
    wv,
    wri,
    wag,
    wrg,
    taps_ref,
    gr_ref,
    gi_ref,
    rate_ref,
    q_out,
    kv_out,
    ag_out,
    rg_out,
    prod_out,
    state_out,
    ends_out,
    w_buf,
    x_all,
    q_pack,
    kv_pack,
    ri_buf,
    tail_buf,
    early_buf,
    my_end,
    wsem,
    xs,
    xr,
    qs,
    qr,
    ks,
    kr,
    as_,
    ar,
    bs,
    br,
    hs,
    hr,
    es,
    er,
):
    me, col = lax.axis_index("sp"), lax.axis_index("tp")
    plane = sp // heads
    lanes = plane // 2
    z, r = lax.div(me, plane), lax.rem(me, plane)
    part_rows = tok_ref.shape[0]
    rows, width = prod_out.shape
    qw = q_out.shape[3]
    kvw = kv_out.shape[4]
    weights = [pltpu.make_async_copy(w, w_buf.at[n], wsem.at[n]) for n, w in enumerate((wq, wk, wv, wri, wag, wrg))]
    for copy in weights:
        copy.start()
    greet("sp", sp)
    greet("tp", tp)
    x_all[col] = rms_rows(tok_ref[...].astype(jnp.float32), ngain_ref[...], EPS_INPUT).astype(jnp.bfloat16)
    pl.semaphore_wait(pltpu.get_barrier_semaphore(), sp + tp - 2)

    def give(k):
        return remote(x_all.at[col], x_all.at[col], xs.at[k], xr.at[k], {"tp": lax.rem(col + k, tp)})

    for k in range(1, tp):
        give(k).start()

    def dot(t, n):
        return jnp.dot(x_all[t], w_buf[n], preferred_element_type=jnp.float32).astype(jnp.bfloat16)

    def spread(k, s, t):
        there = {"sp": lax.rem(z + k, heads) * plane + r}
        n = k * tp + s
        g = lax.rem(z + k, heads)
        return (
            remote(kv_pack.at[g, s], kv_out.at[r, z, t], ks.at[n], kr.at[n], there),
            remote(q_pack.at[g, s], q_out.at[z, t], qs.at[n], qr.at[n], there),
        )

    def across(m, k, s, t):
        src = kv_out.at[r, lax.rem(z - k + heads, heads), t]
        n = (m * heads + k) * tp + s
        return remote(src, src, as_.at[n], ar.at[n], {"sp": z * plane + lax.rem(r + 2 * m, plane)})

    def twin(m, k, s, t):
        src = kv_out.at[lax.rem(r - 2 * m + plane, plane), lax.rem(z - k + heads, heads), t]
        n = (m * heads + k) * tp + s
        return remote(src, src, bs.at[n], br.at[n], {"sp": z * plane + r + 1 - 2 * lax.rem(r, 2)})

    def loop(low, high, fn):
        def one(m, _):
            fn(m)
            return 0

        lax.fori_loop(low, high, one, 0)

    def service(s, t):
        for k in range(heads):
            if k:
                spread(k, s, t)[0].wait_recv()
            loop(1, lanes, lambda m: across(m, k, s, t).start())
            twin(0, k, s, t).start()

    turns = [lax.rem(col - s + tp, tp) for s in range(tp)]
    for s, t in enumerate(turns):
        if s:
            give(s).wait_recv()
        at = pl.ds(pl.multiple_of(t * part_rows, part_rows), part_rows)
        for n in range(3):
            if s == 0:
                weights[n].wait()
            piece = dot(t, n)
            for g in range(heads):
                block = piece[:, g * qw : (g + 1) * qw]
                if n == 0:
                    q_pack[g, s] = block
                else:
                    kv_pack[g, s, :, (n - 1) * qw : n * qw] = block
        kv_out[r, z, t] = kv_pack[z, s]
        q_out[z, t] = q_pack[z, s]
        for k in range(1, heads):
            for copy in spread(k, s, t):
                copy.start()
        if s == 0:
            weights[3].wait()
        ri_buf[at] = dot(t, 3)
        if s:
            service(s - 1, turns[s - 1])
    tail_buf[...] = ri_buf[rows - 16 :]
    halo = remote(tail_buf, early_buf, hs, hr, {"sp": lax.rem(me + 1, sp)})
    halo.start()
    weights[4].wait()
    weights[5].wait()
    for t in range(tp):
        ag_out[t * part_rows : (t + 1) * part_rows] = dot(t, 4)
        rg_out[t * part_rows : (t + 1) * part_rows] = dot(t, 5)
    halo.wait()

    at = lax.broadcasted_iota(jnp.int32, (rows, width), 0)
    taps = taps_ref.shape[0]
    x = ri_buf[...].astype(jnp.float32)
    early = jnp.where(me == 0, 0.0, early_buf[...].astype(jnp.float32))
    conv = x * taps_ref[taps - 1][None]
    for back in range(1, taps):
        moved = pltpu.roll(x, back, 0)
        for row in range(back):
            moved = jnp.where(at == row, early[16 - back + row][None], moved)
        conv = conv + moved * taps_ref[taps - 1 - back][None]
    conv16 = conv.astype(jnp.bfloat16)
    size = gr_ref.shape[1]
    gates, flows = [], []
    for n in range(gr_ref.shape[0]):
        piece = conv16[:, n * size : (n + 1) * size]
        gates.append(jnp.dot(piece, gr_ref[n], preferred_element_type=jnp.float32))
        flows.append(jnp.dot(piece, gi_ref[n], preferred_element_type=jnp.float32))
    recur = jax.nn.sigmoid(jnp.concatenate(gates, axis=1))
    inflow = jax.nn.sigmoid(jnp.concatenate(flows, axis=1))
    log_decay = -RATE_SCALE * recur * rate_ref[...]
    a = jnp.exp(log_decay)
    norm_in = jnp.where((at == 0) & (me == 0), 1.0, jnp.sqrt(fall_of(2.0 * log_decay)))
    b = norm_in * inflow * conv16.astype(jnp.float32)
    shift = 1
    while shift < rows:
        keep = at >= shift
        pa = jnp.where(keep, pltpu.roll(a, shift, 0), 1.0)
        pb = jnp.where(keep, pltpu.roll(b, shift, 0), 0.0)
        b = b + a * pb
        a = a * pa
        shift *= 2
    prod_out[...] = a
    state_out[...] = b
    my_end[...] = jnp.zeros(my_end.shape, jnp.float32)
    my_end[0:1] = a[rows - 1 :]
    my_end[1:2] = b[rows - 1 :]
    ends_out[me] = my_end[...]

    def end(k):
        return remote(my_end, ends_out.at[me], es.at[k], er.at[k], {"sp": lax.rem(me + k, sp)})

    loop(1, sp, lambda k: end(k).start())
    service(tp - 1, turns[tp - 1])
    for s, t in enumerate(turns):
        for k in range(heads):

            def on(m):
                across(m, k, s, t).wait_recv()
                twin(m, k, s, t).start()

            loop(1, lanes, on)
    for s, t in enumerate(turns):
        for k in range(heads):
            if k:
                kv_copy, q_copy = spread(k, s, t)
                kv_copy.wait_send()
                q_copy.wait()
            loop(1, lanes, lambda m: across(m, k, s, t).wait_send())
            loop(0, lanes, lambda m: twin(m, k, s, t).wait())
    for k in range(1, tp):
        give(k).wait_send()
    loop(1, sp, lambda k: end(k).wait())


def back_kernel(
    tp,
    sp,
    heads,
    lam_ref,
    q_ref,
    kv_ref,
    ag_ref,
    rg_ref,
    prod_ref,
    state_ref,
    ends_ref,
    gain_ref,
    oa_hbm,
    or_hbm,
    out_ref,
    oa,
    orr,
    m_ref,
    l_ref,
    acc_ref,
    o_stage,
    o_all,
    rec_part,
    p_stage,
    p_all,
    wsem,
    osd,
    ord_,
    ps,
    pr,
):
    me, col = lax.axis_index("sp"), lax.axis_index("tp")
    plane = sp // heads
    z, r = lax.div(me, plane), lax.rem(me, plane)
    part_rows = q_ref.shape[2]
    rows = tp * part_rows
    width = q_ref.shape[3]
    half = width // 2
    w1 = pltpu.make_async_copy(oa_hbm, oa, wsem.at[0])
    w2 = pltpu.make_async_copy(or_hbm, orr, wsem.at[1])
    w1.start()
    w2.start()
    barrier = pltpu.get_barrier_semaphore()
    for k in range(1, heads):
        pl.semaphore_signal(
            barrier, inc=1, device_id={"sp": lax.rem(z + k, heads) * plane + r}, device_id_type=MESH
        )
    greet("tp", tp)
    pl.semaphore_wait(barrier, heads + tp - 2)
    lane = lax.broadcasted_iota(jnp.int32, (rows, width), 1)

    def give(k):
        g = lax.rem(z + k, heads)
        return remote(o_stage.at[g], o_all.at[z], osd.at[k], ord_.at[k], {"sp": g * plane + r})

    def attend(g):
        mine = g * plane + r
        q = q_ref[g].reshape(rows, width).astype(jnp.float32) * (half ** (-0.5))
        both = (
            jnp.where(lane < half, q, 0.0).astype(jnp.bfloat16),
            jnp.where(lane >= half, q, 0.0).astype(jnp.bfloat16),
        )
        m_ref[...] = jnp.full(m_ref.shape, MASKED, jnp.float32)
        l_ref[...] = jnp.zeros(l_ref.shape, jnp.float32)
        acc_ref[...] = jnp.zeros(acc_ref.shape, jnp.float32)

        def step(pair, masked):
            first = 2 * pair
            at, zz = lax.rem(first, plane), lax.div(first, plane)
            block = kv_ref[pl.ds(at, 2), zz].reshape(2 * rows, -1)
            keys, vals = block[:, :width], block[:, width:]
            scores = [
                lax.dot_general(
                    q_p, keys, (((1,), (1,)), ((), ())), preferred_element_type=jnp.float32
                )
                for q_p in both
            ]
            for p, s in enumerate(scores):
                if masked:
                    qpos = lax.broadcasted_iota(jnp.int32, s.shape, 0) + mine * rows
                    kpos = lax.broadcasted_iota(jnp.int32, s.shape, 1) + first * rows
                    s = jnp.where(kpos <= qpos, s, MASKED)
                old = m_ref[p]
                new = jnp.maximum(old, jnp.max(s, axis=-1, keepdims=True))
                factor = jnp.exp(old - new)
                e = jnp.exp(s - new[:, :1])
                m_ref[p] = new
                part = e[:, :128]
                for c in range(1, s.shape[1] // 128):
                    part = part + e[:, c * 128 : (c + 1) * 128]
                l_ref[p] = l_ref[p] * factor + part
                acc_ref[p] = acc_ref[p] * factor + jnp.dot(
                    e.astype(jnp.bfloat16), vals, preferred_element_type=jnp.float32
                )

        def body(pair, _):
            step(pair, False)
            return 0

        last = lax.div(mine, 2)
        lax.fori_loop(0, last, body, 0)
        step(last, True)
        maps = [acc_ref[p] / jnp.sum(l_ref[p], axis=-1, keepdims=True) for p in range(2)]
        per_head = maps[0] - lam_ref[z] * maps[1]
        normal = rms_rows(per_head, gain_ref[pl.ds(z, 1)], EPS_HEAD) * HEAD_FACTOR
        return normal.astype(jnp.bfloat16)

    for k in list(range(1, heads)) + [0]:
        g = lax.rem(z + k, heads)
        done = attend(g)
        if k:
            o_stage[g] = done
            give(k).start()
        else:
            o_all[z] = done

    def hop(position, carry):
        longer = ends_ref[position, 0:1] * carry + ends_ref[position, 1:2]
        return jnp.where(position < me, longer, carry)

    carry = lax.fori_loop(0, sp - 1, hop, jnp.zeros((1, prod_ref.shape[1]), jnp.float32))
    states = state_ref[...] + prod_ref[...] * carry
    rec = (states * jax.nn.silu(rg_ref[...].astype(jnp.float32))).astype(jnp.bfloat16)
    w1.wait()
    w2.wait()
    rec_part[...] = jnp.dot(rec, orr[...], preferred_element_type=jnp.float32)
    for k in range(1, heads):
        give(k).wait()

    def partial(t):
        at = pl.ds(pl.multiple_of(t * part_rows, part_rows), part_rows)
        att = jnp.concatenate([o_all[h, at] for h in range(heads)], axis=1).astype(jnp.float32)
        mixed = (att * jax.nn.silu(ag_ref[at].astype(jnp.float32))).astype(jnp.bfloat16)
        return rec_part[at] + jnp.dot(mixed, oa[...], preferred_element_type=jnp.float32)

    def pass_on(k):
        t = lax.rem(col + k, tp)
        return remote(p_stage.at[t], p_all.at[col], ps.at[k], pr.at[k], {"tp": t})

    for k in range(1, tp):
        t = lax.rem(col + k, tp)
        p_stage[t] = partial(t).astype(jnp.bfloat16)
        pass_on(k).start()
    total = partial(col)
    for k in range(1, tp):
        pass_on(k).wait()
        total = total + p_all[lax.rem(col - k + tp, tp)].astype(jnp.float32)
    out_ref[...] = total.astype(jnp.bfloat16)


def body(
    tokens,
    norm_gain,
    w_query,
    w_key,
    w_value,
    w_att_gate,
    w_rec_in,
    w_rec_gate,
    conv_taps,
    gate_recur,
    gate_input,
    decay_rate,
    head_lambda,
    head_gain,
    out_att,
    out_rec,
):
    tp, sp, heads = lax.axis_size("tp"), lax.axis_size("sp"), head_lambda.shape[0]
    plane = sp // heads
    lanes = plane // 2
    part, depth = tokens.shape
    rows, width = part * tp, w_query.shape[1]
    qw, vdim = width // heads, w_value.shape[1] // heads
    kvw = qw + vdim
    chans = w_rec_in.shape[1]
    f32, b16 = jnp.float32, jnp.bfloat16
    shape = jax.ShapeDtypeStruct
    dma = pltpu.SemaphoreType.DMA
    steps = heads * tp
    q, kv, ag, rg, prod, state, ends = pl.pallas_call(
        functools.partial(front_kernel, tp, sp, heads),
        out_shape=[
            shape((heads, tp, part, qw), b16),
            shape((plane, heads, tp, part, kvw), b16),
            shape((rows, width), b16),
            shape((rows, chans), b16),
            shape((rows, chans), f32),
            shape((rows, chans), f32),
            shape((sp, 8, chans), f32),
        ],
        in_specs=[VMEM] * 2 + [ANY] * 6 + [VMEM] * 4,
        out_specs=[VMEM] * 7,
        scratch_shapes=[
            pltpu.VMEM((6, depth, width), b16),
            pltpu.VMEM((tp, part, depth), b16),
            pltpu.VMEM((heads, tp, part, qw), b16),
            pltpu.VMEM((heads, tp, part, kvw), b16),
            pltpu.VMEM((rows, chans), b16),
            pltpu.VMEM((16, chans), b16),
            pltpu.VMEM((16, chans), b16),
            pltpu.VMEM((8, chans), f32),
            dma((6,)),
            dma((tp,)),
            dma((tp,)),
            dma((steps,)),
            dma((steps,)),
            dma((steps,)),
            dma((steps,)),
            dma((lanes * steps,)),
            dma((lanes * steps,)),
            dma((lanes * steps,)),
            dma((lanes * steps,)),
            dma,
            dma,
            dma((sp,)),
            dma((sp,)),
        ],
        compiler_params=pltpu.CompilerParams(
            collective_id=0, has_side_effects=True, vmem_limit_bytes=LIMIT
        ),
        name="front",
    )(
        tokens,
        norm_gain.reshape(1, depth),
        w_query,
        w_key,
        w_value,
        w_rec_in,
        w_att_gate,
        w_rec_gate,
        conv_taps,
        gate_recur,
        gate_input,
        decay_rate.reshape(1, chans),
    )
    return pl.pallas_call(
        functools.partial(back_kernel, tp, sp, heads),
        out_shape=shape((part, out_att.shape[1]), b16),
        in_specs=[SMEM] + [VMEM] * 8 + [ANY] * 2,
        out_specs=VMEM,
        scratch_shapes=[
            pltpu.VMEM(out_att.shape, b16),
            pltpu.VMEM(out_rec.shape, b16),
            pltpu.VMEM((2, rows, 128), f32),
            pltpu.VMEM((2, rows, 128), f32),
            pltpu.VMEM((2, rows, vdim), f32),
            pltpu.VMEM((heads, rows, vdim), b16),
            pltpu.VMEM((heads, rows, vdim), b16),
            pltpu.VMEM((rows, out_att.shape[1]), f32),
            pltpu.VMEM((tp, part, out_att.shape[1]), b16),
            pltpu.VMEM((tp, part, out_att.shape[1]), b16),
            dma((2,)),
            dma((heads,)),
            dma((heads,)),
            dma((tp,)),
            dma((tp,)),
        ],
        compiler_params=pltpu.CompilerParams(
            collective_id=1, has_side_effects=True, vmem_limit_bytes=LIMIT
        ),
        name="back",
    )(head_lambda, q, kv, ag, rg, prod, state, ends, head_gain.reshape(heads, vdim), out_att, out_rec)


def solution(mesh):
    return jax.shard_map(
        body,
        mesh=mesh,
        in_specs=(
            P(("sp", "tp"), None),
            P(),
            P(None, "tp"),
            P(None, "tp"),
            P(None, "tp"),
            P(None, "tp"),
            P(None, "tp"),
            P(None, "tp"),
            P(None, "tp"),
            P("tp", None, None),
            P("tp", None, None),
            P("tp"),
            P("tp"),
            P("tp"),
            P("tp", None),
            P("tp", None),
        ),
        out_specs=P(("sp", "tp"), None),
        check_vma=False,
    )
```

time: 301 us -> 80.5 us (0.27)
  local copies, waits for them, and re-layouts: 89.6 us -> 1.88 us
  Pallas kernels: 0 us -> 77.7 us
  matrix products: 67.2 us -> 0 us
  other arithmetic: 43.6 us -> 0 us
  blocking collectives: 42.2 us -> 0 us
  waiting for transfers between devices: 32 us -> 0 us
  between operations: 14.3 us -> 0.02 us
  starting transfers between devices: 8.62 us -> 0 us
    pallas_call x0 -> x2, Pallas kernels: none -> 77.7 us  [the longest x1 43.2 us: body(): pl.pallas_call(functools.partial(front_kernel, tp, sp, heads), out_shape=...]
    dot_general x21 -> x0, matrix products: 67.2 us -> none  [the longest x8 31.2 us: one_block(): jnp.einsum('qhpd,khpd->phqk', query_heads, key_block, preferred_element_t...]
    all_gather x2 -> x0, blocking collectives: 42.2 us -> none  [carried_in(): pieces = jax.tree.map(lambda part: lax.all_gather(part, axis), value)]
    convert_element_type x11 -> x0, other arithmetic: 30.2 us -> none  [the longest x8 26.7 us: one_block(): raised.astype(jnp.bfloat16)]
    unnamed x51 -> x1, local copies, waits for them, and re-layouts: 30 us -> 1.88 us
    reshape x3 -> x0, local copies, waits for them, and re-layouts: 23.3 us -> none  [the longest x1 16.1 us: attention(): key_piece.reshape(block_count, block_len, local_heads, 2, head_dim)]
    dynamic_slice x39 -> x0, local copies, waits for them, and re-layouts: 22.7 us -> none  [the longest x24 22.5 us: attention(): lax.scan(one_block, running, (key_blocks, value_blocks, block_starts))]
    all_gather x5 -> x0, waiting for transfers between devices: 22.6 us -> none  [the longest x1 12.8 us: body(): lax.all_gather(normed, 'tp', axis=0, tiled=True)]
  transfers between devices with their start and end apart: 8 -> 0, of which waited for: 5 -> 0; matrix products, arithmetic and copies ran while one was open for 60% -> 0% of each run, Pallas kernels for 0% -> 0%
where the time goes in v2:
time: 80.5 us; the launch traced here: 79.6 us
  Pallas kernels  77.7 us (97%)
  local copies, waits for them, and re-layouts  1.88 us (2%)
    pallas_call x1, Pallas kernels, body(): pl.pallas_call(functools.partial(front_kernel, tp, sp, heads), out_shape=...  43.2 us
    pallas_call x1, Pallas kernels, body(): pl.pallas_call(functools.partial(back_kernel, tp, sp, heads), out_shape=s...  34.5 us
    unnamed x1, local copies, waits for them, and re-layouts  1.88 us

profile of v2, /device:TPU:0, one launch (start us, length us, event | category | flops | bytes accessed | tf_op | source)
XLA Modules:
  0.0 79.6 jit_solution(15334237906466993143)
XLA Ops:
  0.0 43.2 %front.1 = (bf16[4,2,128,128]{3,2,1,0:T(8,128)(2,1)}, bf16[4,4,2,128,256]{4,3,2,1,0:T(8,128)(2,1)}, bf16[256,512]{1,0:T(8,128)(2,1)}, bf16[256,512]{1,0:T(8,128)...) custom-call(bf16[128,2048]{1,0:T(8,128)(2,1)} %tok_ref.1, f32[1,2048]{1,0:T(1,128)} %bitcast.3, ...), custom_call_target="tpu_custom_call" | custom-call | tf_op jit(solution)/shard_map/front/pallas_call | solution.py:438
  43.2 34.5 %back.1 = bf16[128,2048]{1,0:T(8,128)(2,1)} custom-call(f32[4]{0:T(128)} %lam_ref.1, bf16[4,2,128,128]{3,2,1,0:T(8,128)(2,1)} %get-tuple-element.12.q_ref, bf16[4,4,2,128,256]{4,3,2,1,0:T(8,128)(2,1)} %get-tuple-element.13.kv_ref, bf16[256,512]{1,0:T(8,128)(2,1)} %get-tuple-element.14.ag_ref, bf16[256,512]{1,0:T(8,128)(2,1)} %get-tuple-element.15.rg_ref, ...), custom_call_target="tpu_custom_call" | custom-call | tf_op jit(solution)/shard_map/back/pallas_call | solution.py:494
  77.7 1.9 %copy.18 = bf16[128,2048]{1,0:T(8,128)(2,1)} copy(bf16[128,2048]{1,0:T(8,128)(2,1)} %back.1) | data formatting | bytes 1048576

commit v3 on v2

--- a/solution.py
+++ b/solution.py
@@ -1,4 +1,5 @@
 import functools
+import math
 
 import jax
 import jax.numpy as jnp
@@ -54,6 +55,7 @@
     tp,
     sp,
     heads,
+    begin,
     tok_ref,
     ngain_ref,
     wq,
@@ -108,6 +110,7 @@
     weights = [pltpu.make_async_copy(w, w_buf.at[n], wsem.at[n]) for n, w in enumerate((wq, wk, wv, wri, wag, wrg))]
     for copy in weights:
         copy.start()
+    begin(True)
     greet("sp", sp)
     greet("tp", tp)
     x_all[col] = rms_rows(tok_ref[...].astype(jnp.float32), ngain_ref[...], EPS_INPUT).astype(jnp.bfloat16)
@@ -159,6 +162,8 @@
     for s, t in enumerate(turns):
         if s:
             give(s).wait_recv()
+        if s == tp - 1:
+            begin(False)
         at = pl.ds(pl.multiple_of(t * part_rows, part_rows), part_rows)
         for n in range(3):
             if s == 0:
@@ -254,38 +259,35 @@
     loop(1, sp, lambda k: end(k).wait())
 
 
-def back_kernel(
-    tp,
-    sp,
-    heads,
-    lam_ref,
-    q_ref,
-    kv_ref,
-    ag_ref,
-    rg_ref,
-    prod_ref,
-    state_ref,
-    ends_ref,
-    gain_ref,
-    oa_hbm,
-    or_hbm,
-    out_ref,
-    oa,
-    orr,
-    m_ref,
-    l_ref,
-    acc_ref,
-    o_stage,
-    o_all,
-    rec_part,
-    p_stage,
-    p_all,
-    wsem,
-    osd,
-    ord_,
-    ps,
-    pr,
-):
+def layer_kernel(tp, sp, heads, *refs):
+    lam_ref, gain_ref, oa_hbm, or_hbm, out_ref = refs[12:17]
+    held, front_scratch = refs[17:24], refs[24:47]
+    (
+        oa,
+        orr,
+        m_ref,
+        l_ref,
+        acc_ref,
+        o_stage,
+        o_all,
+        rec_part,
+        p_stage,
+        p_all,
+        a_stage,
+        a_all,
+        wsem,
+        osd,
+        ord_,
+        ps,
+        pr,
+        as_,
+        ar,
+        ws,
+        wr,
+        vs,
+        vr,
+    ) = refs[47:]
+    q_ref, kv_ref, ag_ref, rg_ref, prod_ref, state_ref, ends_ref = held
     me, col = lax.axis_index("sp"), lax.axis_index("tp")
     plane = sp // heads
     z, r = lax.div(me, plane), lax.rem(me, plane)
@@ -293,18 +295,34 @@
     rows = tp * part_rows
     width = q_ref.shape[3]
     half = width // 2
-    w1 = pltpu.make_async_copy(oa_hbm, oa, wsem.at[0])
+    cut = oa.shape[1] // 2
+    side = pl.ds(pl.multiple_of(lax.rem(me, 2) * cut, cut), cut)
+    w1 = pltpu.make_async_copy(oa_hbm, oa.at[col], wsem.at[0])
     w2 = pltpu.make_async_copy(or_hbm, orr, wsem.at[1])
-    w1.start()
-    w2.start()
-    barrier = pltpu.get_barrier_semaphore()
-    for k in range(1, heads):
-        pl.semaphore_signal(
-            barrier, inc=1, device_id={"sp": lax.rem(z + k, heads) * plane + r}, device_id_type=MESH
-        )
-    greet("tp", tp)
-    pl.semaphore_wait(barrier, heads + tp - 2)
+
+    def share(k):
+        block = oa.at[col, side]
+        return remote(block, block, ws.at[k], wr.at[k], {"tp": lax.rem(col + k, tp)})
+
+    def swap(k):
+        block = oa.at[lax.rem(col - k + tp, tp), side]
+        return remote(block, block, vs.at[k], vr.at[k], {"sp": me + 1 - 2 * lax.rem(me, 2)})
+
+    def begin(early):
+        if early:
+            w1.start()
+            w2.start()
+            return
+        w1.wait()
+        for k in range(1, tp):
+            share(k).start()
+
+    front_kernel(tp, sp, heads, begin, *refs[:12], *held, *front_scratch)
+    for k in range(1, tp):
+        share(k).wait_recv()
+        swap(k).start()
     lane = lax.broadcasted_iota(jnp.int32, (rows, width), 1)
+    group = math.gcd(plane, 4)
 
     def give(k):
         g = lax.rem(z + k, heads)
@@ -321,10 +339,10 @@
         l_ref[...] = jnp.zeros(l_ref.shape, jnp.float32)
         acc_ref[...] = jnp.zeros(acc_ref.shape, jnp.float32)
 
-        def step(pair, masked):
-            first = 2 * pair
+        def step(turn, masked):
+            first = group * turn
             at, zz = lax.rem(first, plane), lax.div(first, plane)
-            block = kv_ref[pl.ds(at, 2), zz].reshape(2 * rows, -1)
+            block = kv_ref[pl.ds(at, group), zz].reshape(group * rows, -1)
             keys, vals = block[:, :width], block[:, width:]
             scores = [
                 lax.dot_general(
@@ -350,11 +368,11 @@
                     e.astype(jnp.bfloat16), vals, preferred_element_type=jnp.float32
                 )
 
-        def body(pair, _):
-            step(pair, False)
+        def body(turn, _):
+            step(turn, False)
             return 0
 
-        last = lax.div(mine, 2)
+        last = lax.div(mine, group)
         lax.fori_loop(0, last, body, 0)
         step(last, True)
         maps = [acc_ref[p] / jnp.sum(l_ref[p], axis=-1, keepdims=True) for p in range(2)]
@@ -362,6 +380,36 @@
         normal = rms_rows(per_head, gain_ref[pl.ds(z, 1)], EPS_HEAD) * HEAD_FACTOR
         return normal.astype(jnp.bfloat16)
 
+    def hop(position, carry):
+        longer = ends_ref[position, 0:1] * carry + ends_ref[position, 1:2]
+        return jnp.where(position < me, longer, carry)
+
+    carry = lax.fori_loop(0, sp - 1, hop, jnp.zeros((1, prod_ref.shape[1]), jnp.float32))
+    states = state_ref[...] + prod_ref[...] * carry
+    rec = (states * jax.nn.silu(rg_ref[...].astype(jnp.float32))).astype(jnp.bfloat16)
+    w2.wait()
+    rec_part[...] = jnp.dot(rec, orr[...], preferred_element_type=jnp.float32)
+
+    def part_of(t):
+        return pl.ds(pl.multiple_of(t * part_rows, part_rows), part_rows)
+
+    def pass_on(k):
+        t = lax.rem(col + k, tp)
+        return remote(p_stage.at[t], p_all.at[col], ps.at[k], pr.at[k], {"tp": t})
+
+    def mixed_on(k):
+        t = lax.rem(col + k, tp)
+        return remote(a_stage.at[t], a_all.at[col], as_.at[k], ar.at[k], {"tp": t})
+
+    def mixed(t):
+        at = part_of(t)
+        att = jnp.concatenate([o_all[h, at] for h in range(heads)], axis=1).astype(jnp.float32)
+        return (att * jax.nn.silu(ag_ref[at].astype(jnp.float32))).astype(jnp.bfloat16)
+
+    for k in range(1, tp):
+        t = lax.rem(col + k, tp)
+        p_stage[t] = rec_part[part_of(t)].astype(jnp.bfloat16)
+        pass_on(k).start()
     for k in list(range(1, heads)) + [0]:
         g = lax.rem(z + k, heads)
         done = attend(g)
@@ -370,38 +418,24 @@
             give(k).start()
         else:
             o_all[z] = done
-
-    def hop(position, carry):
-        longer = ends_ref[position, 0:1] * carry + ends_ref[position, 1:2]
-        return jnp.where(position < me, longer, carry)
-
-    carry = lax.fori_loop(0, sp - 1, hop, jnp.zeros((1, prod_ref.shape[1]), jnp.float32))
-    states = state_ref[...] + prod_ref[...] * carry
-    rec = (states * jax.nn.silu(rg_ref[...].astype(jnp.float32))).astype(jnp.bfloat16)
-    w1.wait()
-    w2.wait()
-    rec_part[...] = jnp.dot(rec, orr[...], preferred_element_type=jnp.float32)
     for k in range(1, heads):
         give(k).wait()
-
-    def partial(t):
-        at = pl.ds(pl.multiple_of(t * part_rows, part_rows), part_rows)
-        att = jnp.concatenate([o_all[h, at] for h in range(heads)], axis=1).astype(jnp.float32)
-        mixed = (att * jax.nn.silu(ag_ref[at].astype(jnp.float32))).astype(jnp.bfloat16)
-        return rec_part[at] + jnp.dot(mixed, oa[...], preferred_element_type=jnp.float32)
-
-    def pass_on(k):
+    for k in range(1, tp):
         t = lax.rem(col + k, tp)
-        return remote(p_stage.at[t], p_all.at[col], ps.at[k], pr.at[k], {"tp": t})
-
-    for k in range(1, tp):
-        t = lax.rem(col + k, tp)
-        p_stage[t] = partial(t).astype(jnp.bfloat16)
-        pass_on(k).start()
-    total = partial(col)
-    for k in range(1, tp):
+        a_stage[t] = mixed(t)
+        mixed_on(k).start()
+    total = rec_part[part_of(col)] + jnp.dot(
+        mixed(col), oa[col], preferred_element_type=jnp.float32
+    )
+    for k in range(1, tp):
+        share(k).wait_send()
+        swap(k).wait()
         pass_on(k).wait()
         total = total + p_all[lax.rem(col - k + tp, tp)].astype(jnp.float32)
+    for k in range(1, tp):
+        c = lax.rem(col - k + tp, tp)
+        mixed_on(k).wait()
+        total = total + jnp.dot(a_all[c], oa[c], preferred_element_type=jnp.float32)
     out_ref[...] = total.astype(jnp.bfloat16)
 
 
@@ -435,20 +469,19 @@
     shape = jax.ShapeDtypeStruct
     dma = pltpu.SemaphoreType.DMA
     steps = heads * tp
-    q, kv, ag, rg, prod, state, ends = pl.pallas_call(
-        functools.partial(front_kernel, tp, sp, heads),
-        out_shape=[
-            shape((heads, tp, part, qw), b16),
-            shape((plane, heads, tp, part, kvw), b16),
-            shape((rows, width), b16),
-            shape((rows, chans), b16),
-            shape((rows, chans), f32),
-            shape((rows, chans), f32),
-            shape((sp, 8, chans), f32),
-        ],
-        in_specs=[VMEM] * 2 + [ANY] * 6 + [VMEM] * 4,
-        out_specs=[VMEM] * 7,
+    return pl.pallas_call(
+        functools.partial(layer_kernel, tp, sp, heads),
+        out_shape=shape((part, out_att.shape[1]), b16),
+        in_specs=[VMEM] * 2 + [ANY] * 6 + [VMEM] * 4 + [SMEM, VMEM, ANY, ANY],
+        out_specs=VMEM,
         scratch_shapes=[
+            pltpu.VMEM((heads, tp, part, qw), b16),
+            pltpu.VMEM((plane, heads, tp, part, kvw), b16),
+            pltpu.VMEM((rows, width), b16),
+            pltpu.VMEM((rows, chans), b16),
+            pltpu.VMEM((rows, chans), f32),
+            pltpu.VMEM((rows, chans), f32),
+            pltpu.VMEM((sp, 8, chans), f32),
             pltpu.VMEM((6, depth, width), b16),
             pltpu.VMEM((tp, part, depth), b16),
             pltpu.VMEM((heads, tp, part, qw), b16),
@@ -472,11 +505,34 @@
             dma,
             dma((sp,)),
             dma((sp,)),
+            pltpu.VMEM((tp, *out_att.shape), b16),
+            pltpu.VMEM(out_rec.shape, b16),
+            pltpu.VMEM((2, rows, 128), f32),
+            pltpu.VMEM((2, rows, 128), f32),
+            pltpu.VMEM((2, rows, vdim), f32),
+            pltpu.VMEM((heads, rows, vdim), b16),
+            pltpu.VMEM((heads, rows, vdim), b16),
+            pltpu.VMEM((rows, out_att.shape[1]), f32),
+            pltpu.VMEM((tp, part, out_att.shape[1]), b16),
+            pltpu.VMEM((tp, part, out_att.shape[1]), b16),
+            pltpu.VMEM((tp, part, width), b16),
+            pltpu.VMEM((tp, part, width), b16),
+            dma((2,)),
+            dma((heads,)),
+            dma((heads,)),
+            dma((tp,)),
+            dma((tp,)),
+            dma((tp,)),
+            dma((tp,)),
+            dma((tp,)),
+            dma((tp,)),
+            dma((tp,)),
+            dma((tp,)),
         ],
         compiler_params=pltpu.CompilerParams(
             collective_id=0, has_side_effects=True, vmem_limit_bytes=LIMIT
         ),
-        name="front",
+        name="layer",
     )(
         tokens,
         norm_gain.reshape(1, depth),
@@ -490,34 +546,11 @@
         gate_recur,
         gate_input,
         decay_rate.reshape(1, chans),
+        head_lambda,
+        head_gain.reshape(heads, vdim),
+        out_att,
+        out_rec,
     )
-    return pl.pallas_call(
-        functools.partial(back_kernel, tp, sp, heads),
-        out_shape=shape((part, out_att.shape[1]), b16),
-        in_specs=[SMEM] + [VMEM] * 8 + [ANY] * 2,
-        out_specs=VMEM,
-        scratch_shapes=[
-            pltpu.VMEM(out_att.shape, b16),
-            pltpu.VMEM(out_rec.shape, b16),
-            pltpu.VMEM((2, rows, 128), f32),
-            pltpu.VMEM((2, rows, 128), f32),
-            pltpu.VMEM((2, rows, vdim), f32),
-            pltpu.VMEM((heads, rows, vdim), b16),
-            pltpu.VMEM((heads, rows, vdim), b16),
-            pltpu.VMEM((rows, out_att.shape[1]), f32),
-            pltpu.VMEM((tp, part, out_att.shape[1]), b16),
-            pltpu.VMEM((tp, part, out_att.shape[1]), b16),
-            dma((2,)),
-            dma((heads,)),
-            dma((heads,)),
-            dma((tp,)),
-            dma((tp,)),
-        ],
-        compiler_params=pltpu.CompilerParams(
-            collective_id=1, has_side_effects=True, vmem_limit_bytes=LIMIT
-        ),
-        name="back",
-    )(head_lambda, q, kv, ag, rg, prod, state, ends, head_gain.reshape(heads, vdim), out_att, out_rec)
 
 
 def solution(mesh):

time: 80.5 us -> 67.4 us (0.84)
  Pallas kernels: 77.7 us -> 65.3 us
    pallas_call x2 -> x1, Pallas kernels: 77.7 us -> 65.3 us  [body(): pl.pallas_call(functools.partial(layer_kernel, tp, sp, heads), out_shape=...]
where the time goes in v3:
time: 67.4 us; the launch traced here: 67.2 us
  Pallas kernels  65.3 us (97%)
  local copies, waits for them, and re-layouts  1.88 us (3%)
    pallas_call x1, Pallas kernels, body(): pl.pallas_call(functools.partial(layer_kernel, tp, sp, heads), out_shape=...  65.3 us
    unnamed x1, local copies, waits for them, and re-layouts  1.88 us

profile of v3, /device:TPU:0, one launch (start us, length us, event | category | flops | bytes accessed | tf_op | source)
XLA Modules:
  0.0 67.2 jit_solution(10523519874997157161)
XLA Ops:
  0.0 65.3 %layer.1 = bf16[128,2048]{1,0:T(8,128)(2,1)} custom-call(bf16[128,2048]{1,0:T(8,128)(2,1)} %refs_0_.1, f32[1,2048]{1,0:T(1,128)} %bitcast.3, bf16[2048,512]{1,0:T(8,128)(2,1)} %refs_2_.1, bf16[2048,512]{1,0:T(8,128)(2,1)} %refs_3_.1, bf16[2048,512]{1,0:T(8,128)(2,1)} %refs_4_.1, bf16[2048,512]{1,0:T(8,128)(2,1)} %refs_5_.1, bf16[2048,512]{1,0:T(8,128)(2,1)} %refs_6_.1, ...), custom_call_target="tpu_custom_call" | custom-call | tf_op jit(solution)/shard_map/layer/pallas_call | solution.py:472
  65.4 1.9 %copy.18 = bf16[128,2048]{1,0:T(8,128)(2,1)} copy(bf16[128,2048]{1,0:T(8,128)(2,1)} %layer.1) | data formatting | bytes 1048576

commit v4 on v3

--- a/solution.py
+++ b/solution.py
@@ -108,8 +108,8 @@
     qw = q_out.shape[3]
     kvw = kv_out.shape[4]
     weights = [pltpu.make_async_copy(w, w_buf.at[n], wsem.at[n]) for n, w in enumerate((wq, wk, wv, wri, wag, wrg))]
-    for copy in weights:
-        copy.start()
+    for n in (1, 2, 0, 3, 4, 5):
+        weights[n].start()
     begin(True)
     greet("sp", sp)
     greet("tp", tp)
@@ -165,7 +165,7 @@
         if s == tp - 1:
             begin(False)
         at = pl.ds(pl.multiple_of(t * part_rows, part_rows), part_rows)
-        for n in range(3):
+        for n in (1, 2, 0):
             if s == 0:
                 weights[n].wait()
             piece = dot(t, n)
@@ -175,11 +175,13 @@
                     q_pack[g, s] = block
                 else:
                     kv_pack[g, s, :, (n - 1) * qw : n * qw] = block
-        kv_out[r, z, t] = kv_pack[z, s]
+            if n == 2:
+                for k in range(1, heads):
+                    spread(k, s, t)[0].start()
+                kv_out[r, z, t] = kv_pack[z, s]
+        for k in range(1, heads):
+            spread(k, s, t)[1].start()
         q_out[z, t] = q_pack[z, s]
-        for k in range(1, heads):
-            for copy in spread(k, s, t):
-                copy.start()
         if s == 0:
             weights[3].wait()
         ri_buf[at] = dot(t, 3)

time: 67.4 us -> 67.4 us (level)
  no operation moved by 1% of the time
where the time goes in v4:
time: 67.4 us; the launch traced here: 67.2 us
  Pallas kernels  65.3 us (97%)
  local copies, waits for them, and re-layouts  1.88 us (3%)
    pallas_call x1, Pallas kernels, body(): pl.pallas_call(functools.partial(layer_kernel, tp, sp, heads), out_shape=...  65.3 us
    unnamed x1, local copies, waits for them, and re-layouts  1.88 us

profile of v4, /device:TPU:0, one launch (start us, length us, event | category | flops | bytes accessed | tf_op | source)
XLA Modules:
  0.0 67.2 jit_solution(10878636934072446691)
XLA Ops:
  0.0 65.3 %layer.1 = bf16[128,2048]{1,0:T(8,128)(2,1)} custom-call(bf16[128,2048]{1,0:T(8,128)(2,1)} %refs_0_.1, f32[1,2048]{1,0:T(1,128)} %bitcast.3, bf16[2048,512]{1,0:T(8,128)(2,1)} %refs_2_.1, bf16[2048,512]{1,0:T(8,128)(2,1)} %refs_3_.1, bf16[2048,512]{1,0:T(8,128)(2,1)} %refs_4_.1, bf16[2048,512]{1,0:T(8,128)(2,1)} %refs_5_.1, bf16[2048,512]{1,0:T(8,128)(2,1)} %refs_6_.1, ...), custom_call_target="tpu_custom_call" | custom-call | tf_op jit(solution)/shard_map/layer/pallas_call | solution.py:474
  65.4 1.9 %copy.18 = bf16[128,2048]{1,0:T(8,128)(2,1)} copy(bf16[128,2048]{1,0:T(8,128)(2,1)} %layer.1) | data formatting | bytes 1048576
